TPU v7x, 32 devices: a whole 2x2x4 slice. The times are simulated.
32 devices in a mesh: grp: 2 (over y), fs: 4 (over z), tp: 4 (over x, core).
Axes of the slice: x: 2, y: 2, z: 4, core: 2. Of those that a mesh axis runs over, the one named last changes fastest.
Arguments:
- tokens: bfloat16 [4096, 2048], P(('grp', 'tp')), parts along dimension 0, may hold values from -6 to 6
- gate_weight: float32 [2, 2048, 5632], P(None, 'fs', 'tp'), may hold values from -0.125 to 0.125
- up_weight: float32 [2, 2048, 5632], P(None, 'fs', 'tp'), may hold values from -0.125 to 0.125
- down_weight: float32 [2, 2048, 5632], P(None, 'fs', 'tp'), may hold values from -0.078125 to 0.078125
- in_gain: float32 [2, 2048], P(None, 'fs'), may hold values from 0.1 to 1.9
- out_gain: float32 [2, 2048], replicated, may hold values from 0.1 to 1.9
Outputs:
- sampler_gate: bfloat16 [4, 2048, 5632], P('grp', None, 'fs'), parts along dimension 0
- sampler_up: bfloat16 [4, 2048, 5632], P('grp', None, 'fs'), parts along dimension 0
- sampler_down: bfloat16 [4, 2048, 5632], P('grp', None, 'fs'), parts along dimension 0
- result: bfloat16 [4096, 2048], P(('grp', 'tp', 'fs')), parts along dimension 0
There are 2 independent parts, one for each index of `grp`. A program takes and returns all parts, laid end to end along the dimension named above; an argument that names none is the same for every part. Nothing has to cross between parts.
All inputs are finite; a program needn't handle non-finite values.
Results may differ from a plain program's by a relative error of at most 0.0073.
Values may be sent and summed in bfloat16 or wider, within the bound.
A program may use at most 192 MiB of HBM per device.

v0:
```python
import jax
import jax.numpy as jnp
from jax import lax
from jax.sharding import PartitionSpec as P

EPS = 1e-06


def normalize(rows):
    return rows * lax.rsqrt(jnp.mean(rows * rows, axis=-1, keepdims=True) + EPS)


def body(tokens, gate_weight, up_weight, down_weight, in_gain, out_gain):
    groups = lax.axis_size("fs")
    rows_all = tokens.shape[0]
    rows_mine = rows_all // groups
    model_width = tokens.shape[1]
    local_rows = gate_weight.shape[1]
    block_width = gate_weight.shape[2] // groups
    residual = lax.dynamic_slice_in_dim(
        tokens, lax.axis_index("fs") * rows_mine, rows_mine, 0
    ).astype(jnp.float32)
    normed = normalize(tokens.astype(jnp.float32)).astype(jnp.bfloat16)
    gates = []
    ups = []
    downs = []
    rounded_state = tokens
    contract_last = (((1,), (1,)), ((), ()))
    for section_idx in range(2):
        scale = in_gain[section_idx][:, None]
        gate_rounded = (scale * gate_weight[section_idx]).astype(jnp.bfloat16)
        up_rounded = (scale * up_weight[section_idx]).astype(jnp.bfloat16)
        down_rounded = down_weight[section_idx].astype(jnp.bfloat16)
        flipped = [
            w.T.reshape(groups, block_width, local_rows)
            for w in (gate_rounded, up_rounded, down_rounded)
        ]
        arrived = (
            lax.all_to_all(flipped[0], "fs", split_axis=0, concat_axis=2, tiled=True),
            lax.all_to_all(flipped[1], "fs", split_axis=0, concat_axis=2, tiled=True),
            lax.all_to_all(flipped[2], "fs", split_axis=0, concat_axis=2, tiled=True),
        )
        thin_rows = [w.reshape(block_width, model_width) for w in arrived]
        sampler_mats = (
            lax.all_gather(thin_rows[0], "tp", axis=0, tiled=True),
            lax.all_gather(thin_rows[1], "tp", axis=0, tiled=True),
            lax.all_gather(thin_rows[2], "tp", axis=0, tiled=True),
        )
        gate_flip, up_flip, down_flip = (sampler_mats[0], sampler_mats[1], sampler_mats[2])
        gates.append(gate_flip.T)
        ups.append(up_flip.T)
        downs.append(down_flip.T)

        def hidden_of(row_block):
            gate_act = lax.dot_general(
                row_block, gate_flip, contract_last, preferred_element_type=jnp.float32
            )
            up_act = lax.dot_general(
                row_block, up_flip, contract_last, preferred_element_type=jnp.float32
            )
            return (jax.nn.silu(gate_act) * up_act).astype(jnp.bfloat16)

        if section_idx == 0:
            hidden = hidden_of(normed)
        else:
            hidden = hidden_of(lax.all_gather(normed, "fs", axis=0, tiled=True))
        mixed = lax.psum_scatter(
            jnp.dot(hidden, down_flip, preferred_element_type=jnp.float32),
            "fs",
            scatter_dimension=0,
            tiled=True,
        )
        rounded_state = (residual + 0.5 * out_gain[section_idx] * normalize(mixed)).astype(
            jnp.bfloat16
        )
        if section_idx == 0:
            residual = rounded_state.astype(jnp.float32)
            normed = normalize(residual).astype(jnp.bfloat16)
    return (jnp.stack(gates), jnp.stack(ups), jnp.stack(downs), rounded_state)


def solution(mesh):
    in_specs = (
        P(("grp", "tp"), None),
        P(None, "fs", "tp"),
        P(None, "fs", "tp"),
        P(None, "fs", "tp"),
        P(None, "fs"),
        P(),
    )
    out_specs = (
        P("grp", None, "fs"),
        P("grp", None, "fs"),
        P("grp", None, "fs"),
        P(("grp", "tp", "fs"), None),
    )
    return jax.shard_map(body, mesh=mesh, in_specs=in_specs, out_specs=out_specs, check_vma=False)
```

profile of v0, /device:TPU:0, one launch (start us, length us, event | category | flops | bytes accessed | tf_op | source)
XLA Modules:
  0.0 632.4 jit_solution(15756863925699655642)
XLA Ops:
  8.0 5.6 fusion.21
  15.8 5.6 fusion.20
  28.6 40.3 %all_to_all.90 = bf16[4,352,512]{2,1,0:T(8,128)(2,1)S(1)} all-to-all(bf16[4,352,512]{2,1,0:T(8,128)(2,1)S(1)} %bitcast.106), channel_id=1, replica_groups=mesh['grp'=2,'fs'=4,'tp'=4] {'fs'}, dimensions={0} | all-to-all | bytes 2883584 | tf_op jit(solution)/shard_map/all_to_all | solution.py:39
  71.6 3.8 copy.29
  76.7 36.3 %all_to_all.91 = bf16[4,352,512]{2,1,0:T(8,128)(2,1)S(1)} all-to-all(bf16[4,352,512]{2,1,0:T(8,128)(2,1)S(1)} %bitcast.127), channel_id=1, replica_groups=mesh['grp'=2,'fs'=4,'tp'=4] {'fs'}, dimensions={0} | all-to-all | bytes 2883584 | tf_op jit(solution)/shard_map/all_to_all | solution.py:41
  115.8 36.3 %all_to_all.92 = bf16[4,352,512]{2,1,0:T(8,128)(2,1)S(1)} all-to-all(bf16[4,352,512]{2,1,0:T(8,128)(2,1)S(1)} %bitcast.105), channel_id=1, replica_groups=mesh['grp'=2,'fs'=4,'tp'=4] {'fs'}, dimensions={0} | all-to-all | bytes 2883584 | tf_op jit(solution)/shard_map/all_to_all | solution.py:40
  155.8 7.7 %fusion.12 = f32[512,1408]{1,0:T(8,128)} fusion(bf16[1408,2048]{1,0:T(8,128)(2,1)} %all-gather.8.cloned.1.call-done, bf16[512,2048]{1,0:T(8,128)(2,1)S(1)} %copy-done.3, f32[512]{0:T(512)S(1)} %add_rsqrt_fusion), kind=kOutput, calls=%fused_computation.28 | convolution fusion | flops 2955935744 | bytes 10749952 | tf_op jit(solution)/shard_map/dot_general | solution.py:55
  163.4 41.3 %all-gather.12.cloned.1.call-done = bf16[1408,2048]{1,0:T(8,128)(2,1)} async-done(((bf16[352,2048]{1,0:T(8,128)(2,1)}), bf16[1408,2048]{1,0:T(8,128)(2,1)}) %all-gather.12.cloned.1.call-update) | async-done | bytes 5767184 | tf_op jit(solution)/shard_map/all_gather | solution.py:46
  204.8 14.0 %fusion.15 = f32[512,2048]{1,0:T(8,128)} fusion(bf16[1408,2048]{1,0:T(8,128)(2,1)} %all-gather.16.cloned.1.call-done, bf16[1408,2048]{1,0:T(8,128)(2,1)} %all-gather.12.cloned.1.call-done, f32[512,1408]{1,0:T(8,128)} %fusion.12, bf16[512,2048]{1,0:T(8,128)(2,1)S(1)} %copy-done.3, f32[512]{0:T(512)S(1)} %add_rsqrt_fusion), kind=kOutput, calls=%fused_computation.29 | convolution fusion | flops 5913051136 | bytes 20711424 | tf_op jit(solution)/shard_map/dot_general | solution.py:68
  224.5 4.2 fusion.4
  228.7 77.9 %all_to_all.93 = bf16[4,352,512]{2,1,0:T(8,128)(2,1)S(1)} all-to-all(bf16[4,352,512]{2,1,0:T(8,128)(2,1)S(1)} %bitcast.107), channel_id=1, replica_groups=mesh['grp'=2,'fs'=4,'tp'=4] {'fs'}, dimensions={0} | all-to-all | bytes 2883584 | tf_op jit(solution)/shard_map/all_to_all | solution.py:39
  309.6 11.2 %reduce-scatter.3.cloned.1.call-done = f32[128,2048]{1,0:T(8,128)} async-done(((f32[512,2048]{1,0:T(8,128)}), f32[128,2048]{1,0:T(8,128)}) %reduce-scatter.3.cloned.1.call-update) | async-done | bytes 1048592 | tf_op jit(solution)/shard_map/reduce_scatter | solution.py:67
  324.9 42.6 %all_to_all.94 = bf16[4,352,512]{2,1,0:T(8,128)(2,1)S(1)} all-to-all(bf16[4,352,512]{2,1,0:T(8,128)(2,1)S(1)} %bitcast.126), channel_id=1, replica_groups=mesh['grp'=2,'fs'=4,'tp'=4] {'fs'}, dimensions={0} | all-to-all | bytes 2883584 | tf_op jit(solution)/shard_map/all_to_all | solution.py:41
  370.2 66.1 %all_to_all.95 = bf16[4,352,512]{2,1,0:T(8,128)(2,1)S(1)} all-to-all(bf16[4,352,512]{2,1,0:T(8,128)(2,1)S(1)} %bitcast.104), channel_id=1, replica_groups=mesh['grp'=2,'fs'=4,'tp'=4] {'fs'}, dimensions={0} | all-to-all | bytes 2883584 | tf_op jit(solution)/shard_map/all_to_all | solution.py:40
  440.5 8.3 %fusion.24 = f32[512,1408]{1,0:T(8,128)} fusion(bf16[512,2048]{1,0:T(8,128)(2,1)} %all-gather.20.cloned.1.call-done, bf16[1408,2048]{1,0:T(8,128)(2,1)} %all-gather.10.cloned.1.call-done), kind=kOutput, calls=%fused_computation.43 | convolution fusion | flops 2952790016 | bytes 10747904 | tf_op jit(solution)/shard_map/dot_general | solution.py:55
  448.8 35.8 %all-gather.18.cloned.1.call-done = bf16[1408,2048]{1,0:T(8,128)(2,1)} async-done(((bf16[352,2048]{1,0:T(8,128)(2,1)}), bf16[1408,2048]{1,0:T(8,128)(2,1)}) %all-gather.18.cloned.1.call-update) | async-done | bytes 5767184 | tf_op jit(solution)/shard_map/all_gather | solution.py:47
  484.6 45.5 %all-gather.14.cloned.1.call-done = bf16[1408,2048]{1,0:T(8,128)(2,1)} async-done(((bf16[352,2048]{1,0:T(8,128)(2,1)}), bf16[1408,2048]{1,0:T(8,128)(2,1)}) %all-gather.14.cloned.1.call-update) | async-done | bytes 5767184 | tf_op jit(solution)/shard_map/all_gather | solution.py:46
  530.1 14.6 %fusion.17 = f32[512,2048]{1,0:T(8,128)} fusion(bf16[1408,2048]{1,0:T(8,128)(2,1)} %all-gather.18.cloned.1.call-done, bf16[512,2048]{1,0:T(8,128)(2,1)} %all-gather.20.cloned.1.call-done, bf16[1408,2048]{1,0:T(8,128)(2,1)} %all-gather.14.cloned.1.call-done, f32[512,1408]{1,0:T(8,128)} %fusion.24), kind=kOutput, calls=%fused_computation.30 | convolution fusion | flops 5909905408 | bytes 20709376 | tf_op jit(solution)/shard_map/dot_general | solution.py:68
  544.7 10.0 %pad_maximum_fusion.1 = bf16[2,2048,1408]{1,2,0:T(8,128)(2,1)} fusion(bf16[1,2048,1408]{1,2,0:T(8,128)(2,1)} %bitcast.133, bf16[1,2048,1408]{1,2,0:T(8,128)(2,1)} %bitcast.130), kind=kLoop, calls=%fused_computation.1 | loop fusion | flops 5767168 | bytes 23068672 | tf_op jit(solution)/shard_map/stack | solution.py:79
  554.7 16.1 %copy.33 = bf16[2,2048,1408]{2,1,0:T(8,128)(2,1)} copy(bf16[2,2048,1408]{1,2,0:T(8,128)(2,1)} %pad_maximum_fusion.1) | data formatting | bytes 23068672
  570.8 9.9 %pad_maximum_fusion = bf16[2,2048,1408]{1,2,0:T(8,128)(2,1)} fusion(bf16[1,2048,1408]{1,2,0:T(8,128)(2,1)} %bitcast.131, bf16[1,2048,1408]{1,2,0:T(8,128)(2,1)} %bitcast.128), kind=kLoop, calls=%fused_computation | loop fusion | flops 5767168 | bytes 23068672 | tf_op jit(solution)/shard_map/stack | solution.py:79
  580.7 15.5 %copy.32 = bf16[2,2048,1408]{2,1,0:T(8,128)(2,1)} copy(bf16[2,2048,1408]{1,2,0:T(8,128)(2,1)} %pad_maximum_fusion) | data formatting | bytes 23068672
  596.1 10.0 %pad_maximum_fusion.2 = bf16[2,2048,1408]{1,2,0:T(8,128)(2,1)} fusion(bf16[1,2048,1408]{1,2,0:T(8,128)(2,1)} %bitcast.132, bf16[1,2048,1408]{1,2,0:T(8,128)(2,1)} %bitcast.129), kind=kLoop, calls=%fused_computation.2 | loop fusion | flops 5767168 | bytes 23068672 | tf_op jit(solution)/shard_map/stack | solution.py:79
  606.1 16.1 %copy.34 = bf16[2,2048,1408]{2,1,0:T(8,128)(2,1)} copy(bf16[2,2048,1408]{1,2,0:T(8,128)(2,1)} %pad_maximum_fusion.2) | data formatting | bytes 23068672
  (63 shorter events, 44.0 us)
Async XLA Ops:
  7.2 148.6 %all-gather.8.cloned.1.call-start = ((), (), s32[]{:S(2)}) async-start(), calls=%async_computation.8 | async-start | bytes 7208960 | tf_op jit(solution)/shard_map/all_gather | solution.py:45
  71.6 91.9 %all-gather.16.cloned.1.call-start = ((), (), s32[]{:S(2)}) async-start(), calls=%async_computation.12 | async-start | bytes 7208960 | tf_op jit(solution)/shard_map/all_gather | solution.py:47
  114.2 1.6 copy-start.1
  115.7 89.1 %all-gather.12.cloned.1.call-start = ((), (), s32[]{:S(2)}) async-start(), calls=%async_computation.10 | async-start | bytes 7208960 | tf_op jit(solution)/shard_map/all_gather | solution.py:46
  153.1 2.1 copy-start.3
  154.7 166.1 %reduce-scatter.3.cloned.1.call-start = ((), (), s32[]{:S(2)}) async-start(), calls=%async_computation.14 | async-start | bytes 5242880 | tf_op jit(solution)/shard_map/reduce_scatter | solution.py:67
  218.8 220.2 %all-gather.10.cloned.1.call-start = ((), (), s32[]{:S(2)}) async-start(), calls=%async_computation.9 | async-start | bytes 7208960 | tf_op jit(solution)/shard_map/all_gather | solution.py:45
  307.7 1.8 copy-start.4
  309.2 15.7 %copy-start.2 = (bf16[1,512,1408]{1,2,0:T(8,128)(2,1)S(1)}, bf16[1,512,1408]{1,2,0:T(8,128)(2,1)}, u32[]{:S(2)}) copy-start(bf16[1,512,1408]{1,2,0:T(8,128)(2,1)} %get-tuple-element.15) | copy-start | bytes 4325380
  309.3 131.2 %all-gather.20.cloned.1.call-start = ((), (), s32[]{:S(2)}) async-start(), calls=%async_computation.15 | async-start | bytes 2621440 | tf_op jit(solution)/shard_map/all_gather | solution.py:66
  324.9 159.7 %all-gather.18.cloned.1.call-start = ((), (), s32[]{:S(2)}) async-start(), calls=%async_computation.13 | async-start | bytes 7208960 | tf_op jit(solution)/shard_map/all_gather | solution.py:47
  368.6 1.6 copy-start
  370.1 160.0 %all-gather.14.cloned.1.call-start = ((), (), s32[]{:S(2)}) async-start(), calls=%async_computation.11 | async-start | bytes 7208960 | tf_op jit(solution)/shard_map/all_gather | solution.py:46
  438.9 183.3 %reduce-scatter.5.cloned.1.call-start = ((), (), s32[]{:S(2)}) async-start(), calls=%async_computation.16 | async-start | bytes 5242880 | tf_op jit(solution)/shard_map/reduce_scatter | solution.py:67
Sparse Core Ops, SparseCore 0:
  71.7 42.5 all-gather.7
  115.8 43.3 all-gather.15
  161.4 43.3 all-gather.11
  218.9 101.7 reduce-scatter.2
  322.7 48.3 all-gather.9
  373.1 67.3 all-gather.19
  442.1 42.4 all-gather.17
  486.7 43.3 all-gather.13
  544.8 76.7 reduce-scatter.4
where the time goes:
time: 635 us; the launch traced here: 632 us
  blocking collectives  299 us (47%)
  waiting for transfers between devices  136 us (21%)
  local copies, waits for them, and re-layouts  92.2 us (15%)
  other arithmetic  46 us (7%)
  matrix products  44.5 us (7%)
  between operations  14 us (2%)
    all_to_all x2, blocking collectives, body(): lax.all_to_all(flipped[0], 'fs', split_axis=0, concat_axis=2, tiled=True)  118 us
    all_to_all x2, blocking collectives, body(): lax.all_to_all(flipped[1], 'fs', split_axis=0, concat_axis=2, tiled=True)  102 us
    all_gather x2, waiting for transfers between devices, body(): lax.all_gather(thin_rows[1], 'tp', axis=0, tiled=True)  86.9 us
    all_to_all x2, blocking collectives, body(): lax.all_to_all(flipped[2], 'fs', split_axis=0, concat_axis=2, tiled=True)  78.8 us
    unnamed x24, local copies, waits for them, and re-layouts  72.3 us
    all_gather x2, waiting for transfers between devices, body(): lax.all_gather(thin_rows[2], 'tp', axis=0, tiled=True)  35.8 us
    another operation x3, other arithmetic, body(): return (jnp.stack(gates), jnp.stack(ups), jnp.stack(downs), rounded_state)  29.9 us
    dot_general x2, matrix products, body(): jnp.dot(hidden, down_flip, preferred_element_type=jnp.float32)  28.6 us
  transfers between devices with their start and end apart: 9, of which 5 were waited for; matrix products, arithmetic and copies ran while one was open for 20% of the time, Pallas kernels for 0%

commit v1 on v0

--- a/solution.py
+++ b/solution.py
@@ -1,6 +1,10 @@
+import functools
+
 import jax
 import jax.numpy as jnp
 from jax import lax
+from jax.experimental import pallas as pl
+from jax.experimental.pallas import tpu as pltpu
 from jax.sharding import PartitionSpec as P
 
 EPS = 1e-06
@@ -10,7 +14,7 @@
     return rows * lax.rsqrt(jnp.mean(rows * rows, axis=-1, keepdims=True) + EPS)
 
 
-def body(tokens, gate_weight, up_weight, down_weight, in_gain, out_gain):
+def body_plain(tokens, gate_weight, up_weight, down_weight, in_gain, out_gain):
     groups = lax.axis_size("fs")
     rows_all = tokens.shape[0]
     rows_mine = rows_all // groups
@@ -79,6 +83,145 @@
     return (jnp.stack(gates), jnp.stack(ups), jnp.stack(downs), rounded_state)
 
 
+def prep_kernel(blocks, width, part, scaled, where, *refs):
+    if scaled:
+        gain, weight, *outs, flip = refs
+        rows = weight[0] * gain[0]
+    else:
+        weight, *outs, flip = refs
+        rows = weight[0]
+    flip[...] = rows.astype(jnp.bfloat16).T
+    for shift in range(blocks):
+        target = lax.rem(where[0] + shift, blocks)
+        start = pl.multiple_of(target * width + where[1] * part, 16)
+        outs[shift][...] = flip[pl.ds(start, part), :]
+
+
+def prepare(where, weight, gain, layer, blocks, halves):
+    _, rows, cols = weight.shape
+    width = cols // blocks
+    part = width // halves
+    step = 256 if rows % 256 == 0 else rows
+    in_specs = [pl.BlockSpec((1, step, cols), lambda r, where: (layer, r, 0))]
+    args = [weight]
+    if gain is not None:
+        in_specs.insert(0, pl.BlockSpec((1, step, 1), lambda r, where: (layer, r, 0)))
+        args.insert(0, gain)
+    return pl.pallas_call(
+        functools.partial(prep_kernel, blocks, width, part, gain is not None),
+        grid_spec=pltpu.PrefetchScalarGridSpec(
+            num_scalar_prefetch=1,
+            grid=(rows // step,),
+            in_specs=in_specs,
+            out_specs=[pl.BlockSpec((part, step), lambda r, where: (0, r))] * blocks,
+            scratch_shapes=[pltpu.VMEM((cols, step), jnp.bfloat16)],
+        ),
+        out_shape=[jax.ShapeDtypeStruct((part, rows), jnp.bfloat16)] * blocks,
+        cost_estimate=pl.CostEstimate(
+            flops=rows * cols, bytes_accessed=rows * cols * 5, transcendentals=0
+        ),
+    )(where, *args)
+
+
+def join_kernel(blocks, where, *refs):
+    *pieces, out = refs
+    wide = pieces[0].shape[1]
+    for shift in range(blocks):
+        source = lax.rem(where[0] + blocks - shift, blocks)
+        out[:, pl.ds(pl.multiple_of(source * wide, 128), wide)] = pieces[shift][...]
+
+
+def join(where, pieces):
+    blocks = len(pieces)
+    part, wide = pieces[0].shape
+    full = lambda i, where: (0, 0)
+    return pl.pallas_call(
+        functools.partial(join_kernel, blocks),
+        grid_spec=pltpu.PrefetchScalarGridSpec(
+            num_scalar_prefetch=1,
+            grid=(1,),
+            in_specs=[pl.BlockSpec((part, wide), full)] * blocks,
+            out_specs=pl.BlockSpec((part, wide * blocks), full),
+        ),
+        out_shape=jax.ShapeDtypeStruct((part, wide * blocks), jnp.bfloat16),
+        cost_estimate=pl.CostEstimate(
+            flops=0, bytes_accessed=4 * part * wide * blocks, transcendentals=0
+        ),
+    )(where, *pieces)
+
+
+def emit_kernel(flip, *refs):
+    refs[-1][0] = flip[...].T
+
+
+def emit(flip, layer, stacked):
+    hidden, width = flip.shape
+    step = 256
+    in_specs = [pl.BlockSpec((hidden, step), lambda r: (0, r))]
+    args = [flip]
+    aliases = {}
+    if stacked is not None:
+        in_specs.append(pl.BlockSpec(memory_space=pl.ANY))
+        args.append(stacked)
+        aliases = {1: 0}
+    return pl.pallas_call(
+        emit_kernel,
+        grid=(width // step,),
+        in_specs=in_specs,
+        out_specs=pl.BlockSpec((1, step, hidden), lambda r: (layer, r, 0)),
+        out_shape=jax.ShapeDtypeStruct((2, width, hidden), jnp.bfloat16),
+        input_output_aliases=aliases,
+        cost_estimate=pl.CostEstimate(
+            flops=0, bytes_accessed=4 * hidden * width, transcendentals=0
+        ),
+    )(*args)
+
+
+def body(tokens, gate_weight, up_weight, down_weight, in_gain, out_gain):
+    groups = lax.axis_size("fs")
+    halves = lax.axis_size("grp")
+    block_width = gate_weight.shape[2] // groups
+    model_width = tokens.shape[1]
+    if block_width % (16 * halves) or gate_weight.shape[1] % 128 or gate_weight.shape[2] % 128 or model_width % 256:
+        return body_plain(tokens, gate_weight, up_weight, down_weight, in_gain, out_gain)
+    rows_mine = tokens.shape[0] // groups
+    here = lax.axis_index("fs")
+    where = jnp.stack([here, lax.axis_index("grp")]).astype(jnp.int32)
+    gain_column = in_gain[:, :, None]
+    contract_last = (((1,), (1,)), ((), ()))
+    flips = []
+    for layer in range(2):
+        mats = []
+        for weight, gain in ((gate_weight, gain_column), (up_weight, gain_column), (down_weight, None)):
+            pieces = list(prepare(where, weight, gain, layer, groups, halves))
+            for shift in range(1, groups):
+                ring = [(k, (k + shift) % groups) for k in range(groups)]
+                pieces[shift] = lax.ppermute(pieces[shift], "fs", ring)
+            mats.append(lax.all_gather(join(where, pieces), ("tp", "grp"), axis=0, tiled=True))
+        flips.append(mats)
+    residual = lax.dynamic_slice_in_dim(tokens, here * rows_mine, rows_mine, 0).astype(jnp.float32)
+    normed = normalize(tokens.astype(jnp.float32)).astype(jnp.bfloat16)
+    stacked = [None, None, None]
+    for layer in range(2):
+        gate_flip, up_flip, down_flip = flips[layer]
+        stacked = [emit(flip, layer, held) for flip, held in zip(flips[layer], stacked)]
+        if layer:
+            normed = lax.all_gather(normed, "fs", axis=0, tiled=True)
+        gate_act = lax.dot_general(normed, gate_flip, contract_last, preferred_element_type=jnp.float32)
+        up_act = lax.dot_general(normed, up_flip, contract_last, preferred_element_type=jnp.float32)
+        hidden = (jax.nn.silu(gate_act) * up_act).astype(jnp.bfloat16)
+        mixed = lax.psum_scatter(
+            jnp.dot(hidden, down_flip, preferred_element_type=jnp.float32),
+            "fs",
+            scatter_dimension=0,
+            tiled=True,
+        )
+        rounded_state = (residual + 0.5 * out_gain[layer] * normalize(mixed)).astype(jnp.bfloat16)
+        residual = rounded_state.astype(jnp.float32)
+        normed = normalize(residual).astype(jnp.bfloat16)
+    return (*stacked, rounded_state)
+
+
 def solution(mesh):
     in_specs = (
         P(("grp", "tp"), None),

time: 635 us -> 562 us (0.89)
  blocking collectives: 299 us -> 0 us
  waiting for transfers between devices: 136 us -> 357 us
  Pallas kernels: 0 us -> 87.9 us
  local copies, waits for them, and re-layouts: 92.2 us -> 6.04 us
  starting transfers between devices: 0.78 us -> 42.1 us
  other arithmetic: 46 us -> 8.65 us
    all_to_all x6 -> x0, blocking collectives: 299 us -> none  [the longest x2 118 us: body(): lax.all_to_all(flipped[0], 'fs', split_axis=0, concat_axis=2, tiled=True)]
    pallas_call x0 -> x18, Pallas kernels: none -> 87.9 us  [the longest x6 49.7 us: emit(): pl.pallas_call(emit_kernel, grid=(width // step,), in_specs=in_specs, out...]
    all_gather x7, waiting for transfers between devices: 124 us -> 201 us  [the longest x6 160 us: body(): lax.all_gather(join(where, pieces), ('tp', 'grp'), axis=0, tiled=True)]
    ppermute x0 -> x18, waiting for transfers between devices: none -> 74.4 us  [body(): pieces[shift] = lax.ppermute(pieces[shift], 'fs', ring)]
    reduce_scatter x2, waiting for transfers between devices: 11.2 us -> 82.2 us  [body(): lax.psum_scatter(jnp.dot(hidden, down_flip, preferred_element_type=jnp.fl...]
    unnamed x24 -> x42, local copies, waits for them, and re-layouts: 72.3 us -> 4.33 us
    ppermute x0 -> x18, starting transfers between devices: none -> 41.5 us  [body(): pieces[shift] = lax.ppermute(pieces[shift], 'fs', ring)]
    another operation x3 -> x1, other arithmetic: 29.9 us -> 0.55 us  [body(): where = jnp.stack([here, lax.axis_index('grp')]).astype(jnp.int32)]
  transfers between devices with their start and end apart: 9 -> 27, of which waited for: 5 -> 21; matrix products, arithmetic and copies ran while one was open for 20% -> 4% of each run, Pallas kernels for 0% -> 15%
where the time goes in v1:
time: 562 us; the launch traced here: 560 us
  waiting for transfers between devices  357 us (64%)
  Pallas kernels  87.9 us (16%)
  matrix products  44.1 us (8%)
  starting transfers between devices  42.1 us (7%)
  between operations  14 us (2%)
  other arithmetic  8.65 us (2%)
  local copies, waits for them, and re-layouts  6.04 us (1%)
    all_gather x6, waiting for transfers between devices, body(): lax.all_gather(join(where, pieces), ('tp', 'grp'), axis=0, tiled=True)  160 us
    reduce_scatter x2, waiting for transfers between devices, body(): lax.psum_scatter(jnp.dot(hidden, down_flip, preferred_element_type=jnp.fl...  82.2 us
    ppermute x18, waiting for transfers between devices, body(): pieces[shift] = lax.ppermute(pieces[shift], 'fs', ring)  74.4 us
    pallas_call x6, Pallas kernels, emit(): pl.pallas_call(emit_kernel, grid=(width // step,), in_specs=in_specs, out...  49.7 us
    ppermute x18, starting transfers between devices, body(): pieces[shift] = lax.ppermute(pieces[shift], 'fs', ring)  41.5 us
    all_gather x1, waiting for transfers between devices, body(): normed = lax.all_gather(normed, 'fs', axis=0, tiled=True)  40.4 us
    dot_general x2, matrix products, body(): jnp.dot(hidden, down_flip, preferred_element_type=jnp.float32)  28 us
    pallas_call x6, Pallas kernels, prepare(): pl.pallas_call(functools.partial(prep_kernel, blocks, width, part, gain i...  21.7 us
  transfers between devices with their start and end apart: 27, of which 21 were waited for; matrix products, arithmetic and copies ran while one was open for 4% of the time, Pallas kernels for 15%

profile of v1, /device:TPU:0, one launch (start us, length us, event | category | flops | bytes accessed | tf_op | source)
XLA Modules:
  0.0 560.1 jit_solution(5076908277603566524)
XLA Ops:
  23.9 6.9 %collective-permute-done.10.refs_2_ = bf16[176,512]{1,0:T(8,128)(2,1)S(1)} collective-permute-done((bf16[176,512]{1,0:T(8,128)(2,1)}, bf16[176,512]{1,0:T(8,128)(2,1)S(1)}, u32[]{:S(2)}, u32[]{:S(2)}) %collective-permute-start.10) | collective-permute-done | bytes 180256 | tf_op jit(solution)/shard_map/ppermute | solution.py:199
  49.1 6.0 %collective-permute-done.4.refs_2_ = bf16[176,512]{1,0:T(8,128)(2,1)S(1)} collective-permute-done((bf16[176,512]{1,0:T(8,128)(2,1)}, bf16[176,512]{1,0:T(8,128)(2,1)S(1)}, u32[]{:S(2)}, u32[]{:S(2)}) %collective-permute-start.4) | collective-permute-done | bytes 180256 | tf_op jit(solution)/shard_map/ppermute | solution.py:199
  74.4 6.9 %collective-permute-done.16.refs_2_ = bf16[176,512]{1,0:T(8,128)(2,1)S(1)} collective-permute-done((bf16[176,512]{1,0:T(8,128)(2,1)}, bf16[176,512]{1,0:T(8,128)(2,1)S(1)}, u32[]{:S(2)}, u32[]{:S(2)}) %collective-permute-start.16) | collective-permute-done | bytes 180256 | tf_op jit(solution)/shard_map/ppermute | solution.py:199
  85.4 7.7 %fusion.9 = f32[512,1408]{1,0:T(8,128)} fusion(bf16[1408,2048]{1,0:T(8,128)(2,1)} %all-gather.14.cloned.1.call-done.flip, bf16[512,2048]{1,0:T(8,128)(2,1)S(1)} %copy-done, f32[512]{0:T(512)S(1)} %add_rsqrt_fusion), kind=kOutput, calls=%fused_computation.19 | convolution fusion | flops 2955935744 | bytes 10749952 | tf_op jit(solution)/shard_map/dot_general | solution.py:211
  93.1 33.3 %all-gather.10.cloned.1.call-done.flip = bf16[1408,2048]{1,0:T(8,128)(2,1)} async-done(((bf16[176,2048]{1,0:T(8,128)(2,1)}), bf16[1408,2048]{1,0:T(8,128)(2,1)}) %all-gather.10.cloned.1.call-update) | async-done | bytes 5767184 | tf_op jit(solution)/shard_map/all_gather | solution.py:200
  126.4 45.7 %all-gather.18.cloned.1.call-done.flip = bf16[1408,2048]{1,0:T(8,128)(2,1)} async-done(((bf16[176,2048]{1,0:T(8,128)(2,1)}), bf16[1408,2048]{1,0:T(8,128)(2,1)}) %all-gather.18.cloned.1.call-update) | async-done | bytes 5767184 | tf_op jit(solution)/shard_map/all_gather | solution.py:200
  172.0 14.1 %fusion.2 = f32[512,2048]{1,0:T(8,128)} fusion(bf16[1408,2048]{1,0:T(8,128)(2,1)} %all-gather.18.cloned.1.call-done.flip, f32[512,1408]{1,0:T(8,128)} %fusion.9, bf16[1408,2048]{1,0:T(8,128)(2,1)} %all-gather.10.cloned.1.call-done.flip, bf16[512,2048]{1,0:T(8,128)(2,1)S(1)} %copy-done, f32[512]{0:T(512)S(1)} %add_rsqrt_fusion), kind=kOutput, calls=%fused_computation.9 | convolution fusion | flops 5913051136 | bytes 20711424 | tf_op jit(solution)/shard_map/dot_general | solution.py:214
  195.2 7.3 %collective-permute-done.refs_1_ = bf16[176,512]{1,0:T(8,128)(2,1)S(1)} collective-permute-done((bf16[176,512]{1,0:T(8,128)(2,1)}, bf16[176,512]{1,0:T(8,128)(2,1)S(1)}, u32[]{:S(2)}, u32[]{:S(2)}) %collective-permute-start) | collective-permute-done | bytes 180256 | tf_op jit(solution)/shard_map/ppermute | solution.py:199
  202.5 13.3 %collective-permute-done.1.refs_2_ = bf16[176,512]{1,0:T(8,128)(2,1)S(1)} collective-permute-done((bf16[176,512]{1,0:T(8,128)(2,1)}, bf16[176,512]{1,0:T(8,128)(2,1)S(1)}, u32[]{:S(2)}, u32[]{:S(2)}) %collective-permute-start.1) | collective-permute-done | bytes 180256 | tf_op jit(solution)/shard_map/ppermute | solution.py:199
  219.7 54.9 %reduce-scatter.3.cloned.1.call-done = f32[128,2048]{1,0:T(8,128)} async-done(((f32[512,2048]{1,0:T(8,128)}), f32[128,2048]{1,0:T(8,128)}) %reduce-scatter.3.cloned.1.call-update) | async-done | bytes 1048592 | tf_op jit(solution)/shard_map/reduce_scatter | solution.py:213
  292.5 6.1 %collective-permute-done.7.refs_2_ = bf16[176,512]{1,0:T(8,128)(2,1)S(1)} collective-permute-done((bf16[176,512]{1,0:T(8,128)(2,1)}, bf16[176,512]{1,0:T(8,128)(2,1)S(1)}, u32[]{:S(2)}, u32[]{:S(2)}) %collective-permute-start.7) | collective-permute-done | bytes 180256 | tf_op jit(solution)/shard_map/ppermute | solution.py:199
  319.2 6.2 %collective-permute-done.13.refs_2_ = bf16[176,512]{1,0:T(8,128)(2,1)S(1)} collective-permute-done((bf16[176,512]{1,0:T(8,128)(2,1)}, bf16[176,512]{1,0:T(8,128)(2,1)S(1)}, u32[]{:S(2)}, u32[]{:S(2)}) %collective-permute-start.13) | collective-permute-done | bytes 180256 | tf_op jit(solution)/shard_map/ppermute | solution.py:199
  329.1 40.4 %all-gather.20.cloned.1.call-done = bf16[512,2048]{1,0:T(8,128)(2,1)} async-done(((bf16[128,2048]{1,0:T(8,128)(2,1)}), bf16[512,2048]{1,0:T(8,128)(2,1)}) %all-gather.20.cloned.1.call-update) | async-done | bytes 2097168 | tf_op jit(solution)/shard_map/all_gather | solution.py:209
  369.5 8.4 %fusion.21 = f32[512,1408]{1,0:T(8,128)} fusion(bf16[512,2048]{1,0:T(8,128)(2,1)} %all-gather.20.cloned.1.call-done, bf16[1408,2048]{1,0:T(8,128)(2,1)} %all-gather.8.cloned.1.call-done.flip), kind=kOutput, calls=%fused_computation.31 | convolution fusion | flops 2952790016 | bytes 10747904 | tf_op jit(solution)/shard_map/dot_general | solution.py:210
  377.9 36.0 %all-gather.12.cloned.1.call-done.flip = bf16[1408,2048]{1,0:T(8,128)(2,1)} async-done(((bf16[176,2048]{1,0:T(8,128)(2,1)}), bf16[1408,2048]{1,0:T(8,128)(2,1)}) %all-gather.12.cloned.1.call-update) | async-done | bytes 5767184 | tf_op jit(solution)/shard_map/all_gather | solution.py:200
  414.0 45.1 %all-gather.16.cloned.1.call-done.flip = bf16[1408,2048]{1,0:T(8,128)(2,1)} async-done(((bf16[176,2048]{1,0:T(8,128)(2,1)}), bf16[1408,2048]{1,0:T(8,128)(2,1)}) %all-gather.16.cloned.1.call-update) | async-done | bytes 5767184 | tf_op jit(solution)/shard_map/all_gather | solution.py:200
  459.0 13.9 %fusion.3 = f32[512,2048]{1,0:T(8,128)} fusion(bf16[1408,2048]{1,0:T(8,128)(2,1)} %all-gather.16.cloned.1.call-done.flip, f32[512,1408]{1,0:T(8,128)} %fusion.21, bf16[512,2048]{1,0:T(8,128)(2,1)S(1)} %copy-done.20, bf16[1408,2048]{1,0:T(8,128)(2,1)} %all-gather.12.cloned.1.call-done.flip), kind=kOutput, calls=%fused_computation.10 | convolution fusion | flops 5909905408 | bytes 20709376 | tf_op jit(solution)/shard_map/dot_general | solution.py:214
  473.0 8.4 %shard_map.97.refs_0_ = bf16[2,2048,1408]{2,1,0:T(8,128)(2,1)} custom-call(bf16[1408,2048]{1,0:T(8,128)(2,1)} %all-gather.10.cloned.1.call-done.flip), custom_call_target="tpu_custom_call" | custom-call | bytes 11534336 | tf_op jit(solution)/shard_map/pallas_call | solution.py:167
  481.4 8.2 %shard_map.109.refs_0_ = bf16[2,2048,1408]{2,1,0:T(8,128)(2,1)} custom-call(bf16[1408,2048]{1,0:T(8,128)(2,1)} %all-gather.18.cloned.1.call-done.flip), custom_call_target="tpu_custom_call" | custom-call | bytes 11534336 | tf_op jit(solution)/shard_map/pallas_call | solution.py:167
  489.7 8.3 %shard_map.103.refs_0_ = bf16[2,2048,1408]{2,1,0:T(8,128)(2,1)} custom-call(bf16[1408,2048]{1,0:T(8,128)(2,1)} %all-gather.14.cloned.1.call-done.flip), custom_call_target="tpu_custom_call" | custom-call | bytes 11534336 | tf_op jit(solution)/shard_map/pallas_call | solution.py:167
  497.9 8.3 %shard_map.98 = bf16[2,2048,1408]{2,1,0:T(8,128)(2,1)} custom-call(bf16[1408,2048]{1,0:T(8,128)(2,1)} %all-gather.8.cloned.1.call-done.flip, bf16[2,2048,1408]{2,1,0:T(8,128)(2,1)} %shard_map.97.refs_0_), custom_call_target="tpu_custom_call", output_to_operand_aliasing={{}: (1, {})} | custom-call | bytes 11534336 | tf_op jit(solution)/shard_map/pallas_call | solution.py:167
  506.2 8.3 %shard_map.110 = bf16[2,2048,1408]{2,1,0:T(8,128)(2,1)} custom-call(bf16[1408,2048]{1,0:T(8,128)(2,1)} %all-gather.16.cloned.1.call-done.flip, bf16[2,2048,1408]{2,1,0:T(8,128)(2,1)} %shard_map.109.refs_0_), custom_call_target="tpu_custom_call", output_to_operand_aliasing={{}: (1, {})} | custom-call | bytes 11534336 | tf_op jit(solution)/shard_map/pallas_call | solution.py:167
  514.5 8.2 %shard_map.104 = bf16[2,2048,1408]{2,1,0:T(8,128)(2,1)} custom-call(bf16[1408,2048]{1,0:T(8,128)(2,1)} %all-gather.12.cloned.1.call-done.flip, bf16[2,2048,1408]{2,1,0:T(8,128)(2,1)} %shard_map.103.refs_0_), custom_call_target="tpu_custom_call", output_to_operand_aliasing={{}: (1, {})} | custom-call | bytes 11534336 | tf_op jit(solution)/shard_map/pallas_call | solution.py:167
  522.7 27.3 %reduce-scatter.5.cloned.1.call-done = f32[128,2048]{1,0:T(8,128)} async-done(((f32[512,2048]{1,0:T(8,128)}), f32[128,2048]{1,0:T(8,128)}) %reduce-scatter.5.cloned.1.call-update) | async-done | bytes 1048592 | tf_op jit(solution)/shard_map/reduce_scatter | solution.py:213
  (116 shorter events, 117.0 us)
Async XLA Ops:
  7.2 78.2 %all-gather.14.cloned.1.call-start = ((), (), s32[]{:S(2)}) async-start(), calls=%async_computation.5 | async-start | bytes 6488064 | tf_op jit(solution)/shard_map/all_gather | solution.py:200
  16.2 14.6 %collective-permute-start.10 = (bf16[176,512]{1,0:T(8,128)(2,1)}, bf16[176,512]{1,0:T(8,128)(2,1)S(1)}, u32[]{:S(2)}, u32[]{:S(2)}) collective-permute-start(bf16[176,512]{1,0:T(8,128)(2,1)} %get-tuple-element.42), channel_id=1, source_target_pairs={{0,8},{4,12},{8,0},{12,4},{1,9},{5,13},{9,1},{13,5},{2,10},{6,14},... | collective-permute-start | bytes 540680 | tf_op jit(solution)/shard_map/ppermute | solution.py:199
  18.8 12.0 %collective-permute-start.11 = (bf16[176,512]{1,0:T(8,128)(2,1)}, bf16[176,512]{1,0:T(8,128)(2,1)S(1)}, u32[]{:S(2)}, u32[]{:S(2)}) collective-permute-start(bf16[176,512]{1,0:T(8,128)(2,1)} %get-tuple-element.43), channel_id=1, source_target_pairs={{0,12},{4,0},{8,4},{12,8},{1,13},{5,1},{9,5},{13,9},{2,14},{6,2},{... | collective-permute-start | bytes 540680 | tf_op jit(solution)/shard_map/ppermute | solution.py:199
  34.3 92.1 %all-gather.10.cloned.1.call-start = ((), (), s32[]{:S(2)}) async-start(), calls=%async_computation.3 | async-start | bytes 6488064 | tf_op jit(solution)/shard_map/all_gather | solution.py:200
  42.3 12.8 %collective-permute-start.4 = (bf16[176,512]{1,0:T(8,128)(2,1)}, bf16[176,512]{1,0:T(8,128)(2,1)S(1)}, u32[]{:S(2)}, u32[]{:S(2)}) collective-permute-start(bf16[176,512]{1,0:T(8,128)(2,1)} %get-tuple-element.34), channel_id=1, source_target_pairs={{0,8},{4,12},{8,0},{12,4},{1,9},{5,13},{9,1},{13,5},{2,10},{6,14},... | collective-permute-start | bytes 540680 | tf_op jit(solution)/shard_map/ppermute | solution.py:199
  44.0 11.2 %collective-permute-start.5 = (bf16[176,512]{1,0:T(8,128)(2,1)}, bf16[176,512]{1,0:T(8,128)(2,1)S(1)}, u32[]{:S(2)}, u32[]{:S(2)}) collective-permute-start(bf16[176,512]{1,0:T(8,128)(2,1)} %get-tuple-element.35), channel_id=1, source_target_pairs={{0,12},{4,0},{8,4},{12,8},{1,13},{5,1},{9,5},{13,9},{2,14},{6,2},{... | collective-permute-start | bytes 540680 | tf_op jit(solution)/shard_map/ppermute | solution.py:199
  58.7 113.4 %all-gather.18.cloned.1.call-start = ((), (), s32[]{:S(2)}) async-start(), calls=%async_computation.7 | async-start | bytes 6488064 | tf_op jit(solution)/shard_map/all_gather | solution.py:200
  62.3 12.1 %collective-permute-start.15 = (bf16[176,512]{1,0:T(8,128)(2,1)}, bf16[176,512]{1,0:T(8,128)(2,1)S(1)}, u32[]{:S(2)}, u32[]{:S(2)}) collective-permute-start(bf16[176,512]{1,0:T(8,128)(2,1)} %get-tuple-element.49), channel_id=1, source_target_pairs={{0,4},{4,8},{8,12},{12,0},{1,5},{5,9},{9,13},{13,1},{2,6},{6,10},{... | collective-permute-start | bytes 540680 | tf_op jit(solution)/shard_map/ppermute | solution.py:199
  66.8 14.4 %collective-permute-start.16 = (bf16[176,512]{1,0:T(8,128)(2,1)}, bf16[176,512]{1,0:T(8,128)(2,1)S(1)}, u32[]{:S(2)}, u32[]{:S(2)}) collective-permute-start(bf16[176,512]{1,0:T(8,128)(2,1)} %get-tuple-element.50), channel_id=1, source_target_pairs={{0,8},{4,12},{8,0},{12,4},{1,9},{5,13},{9,1},{13,5},{2,10},{6,14},... | collective-permute-start | bytes 540680 | tf_op jit(solution)/shard_map/ppermute | solution.py:199
  69.2 12.0 %collective-permute-start.17 = (bf16[176,512]{1,0:T(8,128)(2,1)}, bf16[176,512]{1,0:T(8,128)(2,1)S(1)}, u32[]{:S(2)}, u32[]{:S(2)}) collective-permute-start(bf16[176,512]{1,0:T(8,128)(2,1)} %get-tuple-element.51), channel_id=1, source_target_pairs={{0,12},{4,0},{8,4},{12,8},{1,13},{5,1},{9,5},{13,9},{2,14},{6,2},{... | collective-permute-start | bytes 540680 | tf_op jit(solution)/shard_map/ppermute | solution.py:199
  84.8 189.9 %reduce-scatter.3.cloned.1.call-start = ((), (), s32[]{:S(2)}) async-start(), calls=%async_computation.8 | async-start | bytes 5242880 | tf_op jit(solution)/shard_map/reduce_scatter | solution.py:213
  186.2 142.9 %all-gather.8.cloned.1.call-start = ((), (), s32[]{:S(2)}) async-start(), calls=%async_computation.2 | async-start | bytes 6488064 | tf_op jit(solution)/shard_map/all_gather | solution.py:200
  189.8 12.6 %collective-permute-start = (bf16[176,512]{1,0:T(8,128)(2,1)}, bf16[176,512]{1,0:T(8,128)(2,1)S(1)}, u32[]{:S(2)}, u32[]{:S(2)}) collective-permute-start(bf16[176,512]{1,0:T(8,128)(2,1)} %get-tuple-element.29), channel_id=1, source_target_pairs={{0,4},{4,8},{8,12},{12,0},{1,5},{5,9},{9,13},{13,1},{2,6},{6,10},{... | collective-permute-start | bytes 540680 | tf_op jit(solution)/shard_map/ppermute | solution.py:199
  191.3 24.4 %collective-permute-start.1 = (bf16[176,512]{1,0:T(8,128)(2,1)}, bf16[176,512]{1,0:T(8,128)(2,1)S(1)}, u32[]{:S(2)}, u32[]{:S(2)}) collective-permute-start(bf16[176,512]{1,0:T(8,128)(2,1)} %get-tuple-element.30), channel_id=1, source_target_pairs={{0,8},{4,12},{8,0},{12,4},{1,9},{5,13},{9,1},{13,5},{2,10},{6,14},... | collective-permute-start | bytes 540680 | tf_op jit(solution)/shard_map/ppermute | solution.py:199
  193.7 22.2 %collective-permute-start.2 = (bf16[176,512]{1,0:T(8,128)(2,1)}, bf16[176,512]{1,0:T(8,128)(2,1)S(1)}, u32[]{:S(2)}, u32[]{:S(2)}) collective-permute-start(bf16[176,512]{1,0:T(8,128)(2,1)} %get-tuple-element.31), channel_id=1, source_target_pairs={{0,12},{4,0},{8,4},{12,8},{1,13},{5,1},{9,5},{13,9},{2,14},{6,2},{... | collective-permute-start | bytes 540680 | tf_op jit(solution)/shard_map/ppermute | solution.py:199
  219.4 150.0 %all-gather.20.cloned.1.call-start = ((), (), s32[]{:S(2)}) async-start(), calls=%async_computation.9 | async-start | bytes 2621440 | tf_op jit(solution)/shard_map/all_gather | solution.py:209
  278.6 135.3 %all-gather.12.cloned.1.call-start = ((), (), s32[]{:S(2)}) async-start(), calls=%async_computation.4 | async-start | bytes 6488064 | tf_op jit(solution)/shard_map/all_gather | solution.py:200
  287.2 11.3 %collective-permute-start.7 = (bf16[176,512]{1,0:T(8,128)(2,1)}, bf16[176,512]{1,0:T(8,128)(2,1)S(1)}, u32[]{:S(2)}, u32[]{:S(2)}) collective-permute-start(bf16[176,512]{1,0:T(8,128)(2,1)} %get-tuple-element.38), channel_id=1, source_target_pairs={{0,8},{4,12},{8,0},{12,4},{1,9},{5,13},{9,1},{13,5},{2,10},{6,14},... | collective-permute-start | bytes 540680 | tf_op jit(solution)/shard_map/ppermute | solution.py:199
  287.4 12.0 %collective-permute-start.8 = (bf16[176,512]{1,0:T(8,128)(2,1)}, bf16[176,512]{1,0:T(8,128)(2,1)S(1)}, u32[]{:S(2)}, u32[]{:S(2)}) collective-permute-start(bf16[176,512]{1,0:T(8,128)(2,1)} %get-tuple-element.39), channel_id=1, source_target_pairs={{0,12},{4,0},{8,4},{12,8},{1,13},{5,1},{9,5},{13,9},{2,14},{6,2},{... | collective-permute-start | bytes 540680 | tf_op jit(solution)/shard_map/ppermute | solution.py:199
  302.9 156.2 %all-gather.16.cloned.1.call-start = ((), (), s32[]{:S(2)}) async-start(), calls=%async_computation.6 | async-start | bytes 6488064 | tf_op jit(solution)/shard_map/all_gather | solution.py:200
  306.4 12.8 %collective-permute-start.12 = (bf16[176,512]{1,0:T(8,128)(2,1)}, bf16[176,512]{1,0:T(8,128)(2,1)S(1)}, u32[]{:S(2)}, u32[]{:S(2)}) collective-permute-start(bf16[176,512]{1,0:T(8,128)(2,1)} %get-tuple-element.45), channel_id=1, source_target_pairs={{0,4},{4,8},{8,12},{12,0},{1,5},{5,9},{9,13},{13,1},{2,6},{6,10},{... | collective-permute-start | bytes 540680 | tf_op jit(solution)/shard_map/ppermute | solution.py:199
  310.8 14.6 %collective-permute-start.13 = (bf16[176,512]{1,0:T(8,128)(2,1)}, bf16[176,512]{1,0:T(8,128)(2,1)S(1)}, u32[]{:S(2)}, u32[]{:S(2)}) collective-permute-start(bf16[176,512]{1,0:T(8,128)(2,1)} %get-tuple-element.46), channel_id=1, source_target_pairs={{0,8},{4,12},{8,0},{12,4},{1,9},{5,13},{9,1},{13,5},{2,10},{6,14},... | collective-permute-start | bytes 540680 | tf_op jit(solution)/shard_map/ppermute | solution.py:199
  314.1 11.4 %collective-permute-start.14 = (bf16[176,512]{1,0:T(8,128)(2,1)}, bf16[176,512]{1,0:T(8,128)(2,1)S(1)}, u32[]{:S(2)}, u32[]{:S(2)}) collective-permute-start(bf16[176,512]{1,0:T(8,128)(2,1)} %get-tuple-element.47), channel_id=1, source_target_pairs={{0,12},{4,0},{8,4},{12,8},{1,13},{5,1},{9,5},{13,9},{2,14},{6,2},{... | collective-permute-start | bytes 540680 | tf_op jit(solution)/shard_map/ppermute | solution.py:199
  329.0 220.9 %reduce-scatter.5.cloned.1.call-start = ((), (), s32[]{:S(2)}) async-start(), calls=%async_computation.10 | async-start | bytes 5242880 | tf_op jit(solution)/shard_map/reduce_scatter | solution.py:213
  (24 other events, 236.3 us)
Sparse Core Ops, SparseCore 0:
  34.4 46.2 all-gather.13
  83.1 43.1 all-gather.9
  128.8 43.1 all-gather.17
  186.3 88.3 reduce-scatter.2
  277.0 44.7 all-gather.7
  323.8 45.6 all-gather.19
  371.9 41.9 all-gather.11
  415.8 43.1 all-gather.15
  473.1 76.7 reduce-scatter.4

commit v2 on v1

--- a/solution.py
+++ b/solution.py
@@ -85,16 +85,16 @@
 
 def prep_kernel(blocks, width, part, scaled, where, *refs):
     if scaled:
-        gain, weight, *outs, flip = refs
+        gain, weight, out, flip = refs
         rows = weight[0] * gain[0]
     else:
-        weight, *outs, flip = refs
+        weight, out, flip = refs
         rows = weight[0]
     flip[...] = rows.astype(jnp.bfloat16).T
-    for shift in range(blocks):
-        target = lax.rem(where[0] + shift, blocks)
-        start = pl.multiple_of(target * width + where[1] * part, 16)
-        outs[shift][...] = flip[pl.ds(start, part), :]
+    skip = where[0] * part if part < width else 0
+    for target in range(blocks):
+        start = pl.multiple_of(target * width + skip, 16)
+        out[target] = flip[pl.ds(start, part), :]
 
 
 def prepare(where, weight, gain, layer, blocks, halves):
@@ -113,41 +113,160 @@
             num_scalar_prefetch=1,
             grid=(rows // step,),
             in_specs=in_specs,
-            out_specs=[pl.BlockSpec((part, step), lambda r, where: (0, r))] * blocks,
+            out_specs=pl.BlockSpec((blocks, part, step), lambda r, where: (0, 0, r)),
             scratch_shapes=[pltpu.VMEM((cols, step), jnp.bfloat16)],
         ),
-        out_shape=[jax.ShapeDtypeStruct((part, rows), jnp.bfloat16)] * blocks,
+        out_shape=jax.ShapeDtypeStruct((blocks, part, rows), jnp.bfloat16),
         cost_estimate=pl.CostEstimate(
             flops=rows * cols, bytes_accessed=rows * cols * 5, transcendentals=0
         ),
     )(where, *args)
 
 
-def join_kernel(blocks, where, *refs):
-    *pieces, out = refs
-    wide = pieces[0].shape[1]
-    for shift in range(blocks):
-        source = lax.rem(where[0] + blocks - shift, blocks)
-        out[:, pl.ds(pl.multiple_of(source * wide, 128), wide)] = pieces[shift][...]
-
-
-def join(where, pieces):
-    blocks = len(pieces)
-    part, wide = pieces[0].shape
-    full = lambda i, where: (0, 0)
+def spread_kernel(blocks, *refs):
+    sources, full = refs[:3], refs[3:6]
+    own, (own_sem, send_sem, recv_sem) = refs[6:9], refs[9:]
+    y, z, t = lax.axis_index("grp"), lax.axis_index("fs"), lax.axis_index("tp")
+    x, c = t // 2, lax.rem(t, 2)
+    other_y, other_x, other_c = 1 - y, (1 - x) * 2 + c, x * 2 + (1 - c)
+    wide = sources[0].shape[-1]
+    partners = [{"fs": lax.rem(z + shift, blocks)} for shift in range(1, blocks)]
+    partners += [{"tp": other_x}, {"tp": other_c}, {"grp": other_y}]
+
+    barrier = pltpu.get_barrier_semaphore()
+    for partner in partners:
+        pl.semaphore_signal(barrier, inc=1, device_id=partner, device_id_type=pl.DeviceIdType.MESH)
+    pl.semaphore_wait(barrier, len(partners))
+
+    def columns(source):
+        return pl.ds(pl.multiple_of(source * wide, 128), wide)
+
+    def place(m, column, half, source):
+        cols = columns(source)
+        if m == 2:
+            return full[m].at[column, :, :, cols]
+        return full[m].at[column, half, :, cols]
+
+    def rows_of(m, column, half):
+        if m == 2:
+            return full[m].at[column]
+        return full[m].at[column, half]
+
+    def origin(m, target):
+        return sources[m].at[target]
+
+    names = []
+    sent = []
+
+    def slot(name):
+        if name not in names:
+            names.append(name)
+        return names.index(name)
+
+    def send(name, source, target, device):
+        k = slot(name)
+        copy = pltpu.make_async_remote_copy(
+            src_ref=source,
+            dst_ref=target,
+            send_sem=send_sem.at[k],
+            recv_sem=recv_sem.at[k],
+            device_id=device,
+            device_id_type=pl.DeviceIdType.MESH,
+        )
+        copy.start()
+        sent.append(copy)
+
+    def arrived(name, landed, device):
+        k = slot(name)
+        pltpu.make_async_remote_copy(
+            src_ref=landed,
+            dst_ref=landed,
+            send_sem=send_sem.at[k],
+            recv_sem=recv_sem.at[k],
+            device_id=device,
+            device_id_type=pl.DeviceIdType.MESH,
+        ).wait_recv()
+
+    to_x, to_c, to_y = {"tp": other_x}, {"tp": other_c}, {"grp": other_y}
+    fetch = []
+    for m in range(3):
+        for shift in range(1, blocks):
+            target = lax.rem(z + shift, blocks)
+            send(("z", m, shift), origin(m, target), place(m, t, y, z), {"fs": target})
+        mine = origin(m, z)
+        send(("x", m, 0), mine, place(m, t, y, z), to_x)
+        if m < 2:
+            send(("y", m, 0, 0), mine, place(m, t, y, z), to_y)
+        copy = pltpu.make_async_copy(mine, own[m], own_sem.at[m])
+        copy.start()
+        fetch.append(copy)
+    kept = []
+    for m in range(3):
+        fetch[m].wait()
+        copy = pltpu.make_async_copy(own[m], place(m, t, y, z), own_sem.at[3 + m])
+        copy.start()
+        kept.append(copy)
+
+    def relay(m, shift):
+        source = lax.rem(z + blocks - shift, blocks)
+        arrived(("x", m, shift), place(m, other_x, y, source), to_x)
+        if m < 2:
+            spot = place(m, other_x, y, source)
+            send(("y", m, 1, shift), spot, spot, to_y)
+
+    for m in range(3):
+        for shift in range(1, blocks):
+            source = lax.rem(z + blocks - shift, blocks)
+            spot = place(m, t, y, source)
+            arrived(("z", m, shift), spot, {"fs": source})
+            send(("x", m, shift), spot, spot, to_x)
+            if m < 2:
+                send(("y", m, 0, shift), spot, spot, to_y)
+            relay(m, shift - 1)
+        kept[m].wait()
+        send(("c", m, 0, 0), rows_of(m, t, y), rows_of(m, t, y), to_c)
+        relay(m, blocks - 1)
+        send(("c", m, 1, 0), rows_of(m, other_x, y), rows_of(m, other_x, y), to_c)
+    for m in range(2):
+        for far, column in ((0, t), (1, other_x)):
+            for shift in range(blocks):
+                source = lax.rem(z + blocks - shift, blocks)
+                arrived(("y", m, far, shift), place(m, column, other_y, source), to_y)
+            rows = rows_of(m, column, other_y)
+            send(("c", m, far, 1), rows, rows, to_c)
+    other_both = (1 - x) * 2 + (1 - c)
+    for m in range(3):
+        for far, column in ((0, other_c), (1, other_both)):
+            arrived(("c", m, far, 0), rows_of(m, column, y), to_c)
+            if m < 2:
+                arrived(("c", m, far, 1), rows_of(m, column, other_y), to_c)
+    for copy in sent:
+        copy.wait_send()
+
+
+def spread(sources, layer, blocks, columns):
+    halves, part = 2, sources[0].shape[1]
+    rows = sources[0].shape[2]
+    sources = [sources[0], sources[1], sources[2].reshape(blocks, halves, part, rows)]
+    count = 3 * (blocks - 1) + 3 * blocks + 4 * blocks + 10
+    shape = (columns, halves, part, rows * blocks)
+    moved = columns * halves * part * rows * blocks * 2
     return pl.pallas_call(
-        functools.partial(join_kernel, blocks),
-        grid_spec=pltpu.PrefetchScalarGridSpec(
-            num_scalar_prefetch=1,
-            grid=(1,),
-            in_specs=[pl.BlockSpec((part, wide), full)] * blocks,
-            out_specs=pl.BlockSpec((part, wide * blocks), full),
-        ),
-        out_shape=jax.ShapeDtypeStruct((part, wide * blocks), jnp.bfloat16),
-        cost_estimate=pl.CostEstimate(
-            flops=0, bytes_accessed=4 * part * wide * blocks, transcendentals=0
-        ),
-    )(where, *pieces)
+        functools.partial(spread_kernel, blocks),
+        in_specs=[pl.BlockSpec(memory_space=pl.ANY)] * 3,
+        out_specs=[pl.BlockSpec(memory_space=pl.ANY)] * 3,
+        out_shape=[jax.ShapeDtypeStruct(shape, jnp.bfloat16)] * 3,
+        scratch_shapes=[
+            pltpu.VMEM((part, rows), jnp.bfloat16),
+            pltpu.VMEM((part, rows), jnp.bfloat16),
+            pltpu.VMEM((halves, part, rows), jnp.bfloat16),
+            pltpu.SemaphoreType.DMA((6,)),
+            pltpu.SemaphoreType.DMA((count,)),
+            pltpu.SemaphoreType.DMA((count,)),
+        ],
+        compiler_params=pltpu.CompilerParams(collective_id=layer, has_side_effects=True),
+        cost_estimate=pl.CostEstimate(flops=0, bytes_accessed=moved * 40, transcendentals=0),
+    )(*sources)
 
 
 def emit_kernel(flip, *refs):
@@ -182,23 +301,24 @@
     halves = lax.axis_size("grp")
     block_width = gate_weight.shape[2] // groups
     model_width = tokens.shape[1]
-    if block_width % (16 * halves) or gate_weight.shape[1] % 128 or gate_weight.shape[2] % 128 or model_width % 256:
+    columns = lax.axis_size("tp")
+    odd = block_width % 32 or gate_weight.shape[1] % 128 or gate_weight.shape[2] % 128
+    if odd or model_width % 256 or halves != 2 or columns != 4:
         return body_plain(tokens, gate_weight, up_weight, down_weight, in_gain, out_gain)
     rows_mine = tokens.shape[0] // groups
     here = lax.axis_index("fs")
-    where = jnp.stack([here, lax.axis_index("grp")]).astype(jnp.int32)
+    where = lax.axis_index("grp")[None].astype(jnp.int32)
     gain_column = in_gain[:, :, None]
     contract_last = (((1,), (1,)), ((), ()))
     flips = []
     for layer in range(2):
-        mats = []
-        for weight, gain in ((gate_weight, gain_column), (up_weight, gain_column), (down_weight, None)):
-            pieces = list(prepare(where, weight, gain, layer, groups, halves))
-            for shift in range(1, groups):
-                ring = [(k, (k + shift) % groups) for k in range(groups)]
-                pieces[shift] = lax.ppermute(pieces[shift], "fs", ring)
-            mats.append(lax.all_gather(join(where, pieces), ("tp", "grp"), axis=0, tiled=True))
-        flips.append(mats)
+        pieces = [
+            prepare(where, gate_weight, gain_column, layer, groups, halves),
+            prepare(where, up_weight, gain_column, layer, groups, halves),
+            prepare(where, down_weight, None, layer, groups, 1),
+        ]
+        whole = spread(pieces, layer, groups, columns)
+        flips.append([mat.reshape(columns * block_width, model_width) for mat in whole])
     residual = lax.dynamic_slice_in_dim(tokens, here * rows_mine, rows_mine, 0).astype(jnp.float32)
     normed = normalize(tokens.astype(jnp.float32)).astype(jnp.bfloat16)
     stacked = [None, None, None]
@@ -211,11 +331,11 @@
         up_act = lax.dot_general(normed, up_flip, contract_last, preferred_element_type=jnp.float32)
         hidden = (jax.nn.silu(gate_act) * up_act).astype(jnp.bfloat16)
         mixed = lax.psum_scatter(
-            jnp.dot(hidden, down_flip, preferred_element_type=jnp.float32),
+            jnp.dot(hidden, down_flip, preferred_element_type=jnp.float32).astype(jnp.bfloat16),
             "fs",
             scatter_dimension=0,
             tiled=True,
-        )
+        ).astype(jnp.float32)
         rounded_state = (residual + 0.5 * out_gain[layer] * normalize(mixed)).astype(jnp.bfloat16)
         residual = rounded_state.astype(jnp.float32)
         normed = normalize(residual).astype(jnp.bfloat16)

time: 562 us -> 394 us (0.70)
  waiting for transfers between devices: 357 us -> 46.8 us
  Pallas kernels: 87.9 us -> 273 us
  starting transfers between devices: 42.1 us -> 0.3 us
    pallas_call x6 -> x2, Pallas kernels: 16.6 us -> 206 us  [spread(): pl.pallas_call(functools.partial(spread_kernel, blocks), in_specs=[pl.Blo...]
    all_gather x6 -> x0, waiting for transfers between devices: 160 us -> none  [body(): lax.all_gather(join(where, pieces), ('tp', 'grp'), axis=0, tiled=True)]
    ppermute x18 -> x0, waiting for transfers between devices: 74.4 us -> none  [body(): pieces[shift] = lax.ppermute(pieces[shift], 'fs', ring)]
    ppermute x18 -> x0, starting transfers between devices: 41.5 us -> none  [body(): pieces[shift] = lax.ppermute(pieces[shift], 'fs', ring)]
    all_gather x1, waiting for transfers between devices: 40.4 us -> 0.02 us  [body(): normed = lax.all_gather(normed, 'fs', axis=0, tiled=True)]
    reduce_scatter x2, waiting for transfers between devices: 82.2 us -> 46.7 us  [body(): lax.psum_scatter(jnp.dot(hidden, down_flip, preferred_element_type=jnp.fl...]
    dot_general x1 -> x2, matrix products: 8.44 us -> 16.1 us  [body(): lax.dot_general(normed, gate_flip, contract_last, preferred_element_type=...]
    dot_general x1 -> x0, matrix products: 7.68 us -> none  [body(): lax.dot_general(normed, up_flip, contract_last, preferred_element_type=jn...]
  transfers between devices with their start and end apart: 27 -> 3, of which waited for: 21 -> 1; matrix products, arithmetic and copies ran while one was open for 4% -> 0% of each run, Pallas kernels for 15% -> 45%
where the time goes in v2:
time: 394 us; the launch traced here: 387 us
  Pallas kernels  273 us (69%)
  waiting for transfers between devices  46.8 us (12%)
  matrix products  42.7 us (11%)
  between operations  13.8 us (4%)
  other arithmetic  9.08 us (2%)
    pallas_call x2, Pallas kernels, spread(): pl.pallas_call(functools.partial(spread_kernel, blocks), in_specs=[pl.Blo...  206 us
    pallas_call x6, Pallas kernels, emit(): pl.pallas_call(emit_kernel, grid=(width // step,), in_specs=in_specs, out...  49.5 us
    reduce_scatter x2, waiting for transfers between devices, body(): lax.psum_scatter(jnp.dot(hidden, down_flip, preferred_element_type=jnp.fl...  46.7 us
    dot_general x2, matrix products, body(): jnp.dot(hidden, down_flip, preferred_element_type=jnp.float32)  26.6 us
    pallas_call x6, Pallas kernels, prepare(): pl.pallas_call(functools.partial(prep_kernel, blocks, width, part, gain i...  17.9 us
    dot_general x2, matrix products, body(): lax.dot_general(normed, gate_flip, contract_last, preferred_element_type=...  16.1 us
  transfers between devices with their start and end apart: 3, of which 1 were waited for; matrix products, arithmetic and copies ran while one was open for 0% of the time, Pallas kernels for 45%

profile of v2, /device:TPU:0, one launch (start us, length us, event | category | flops | bytes accessed | tf_op | source)
XLA Modules:
  0.0 387.3 jit_solution(4010406357447830779)
XLA Ops:
  7.2 2.1 fusion
  9.3 1.7 copy.13.refs_0_
  11.0 3.0 shard_map.98.refs_1_
  14.0 3.0 shard_map.97.refs_0_
  17.0 2.9 shard_map.99
  19.9 89.7 %shard_map.100 = (bf16[4,2,176,2048]{3,2,1,0:T(8,128)(2,1)}, bf16[4,2,176,2048]{3,2,1,0:T(8,128)(2,1)}, bf16[4,2,176,2048]{3,2,1,0:T(8,128)(2,1)}) custom-call(bf16[4,176,512]{2,1,0:T(8,128)(2,1)} %shard_map.97.refs_0_, bf16[4,176,512]{2,1,0:T(8,128)(2,1)} %shard_map.98.refs_1_, bf16[4,2,176,512]{3,2,1,0:T(8,128)(2,1)} %bitcast.27), custom_call_target="tpu_custom_call" | custom-call | bytes 230686720 | tf_op jit(solution)/shard_map/pallas_call | solution.py:254
  109.6 7.7 %fusion.14 = f32[512,1408]{1,0:T(8,128)} fusion(bf16[1408,2048]{1,0:T(8,128)(2,1)} %bitcast.28, bf16[512,2048]{1,0:T(8,128)(2,1)S(1)} %copy-done, f32[512]{0:T(512)S(1)} %add_rsqrt_fusion), kind=kOutput, calls=%fused_computation.26 | convolution fusion | flops 2955935744 | bytes 10749952 | tf_op jit(solution)/shard_map/dot_general | solution.py:330
  117.3 13.3 %convolution_convert_fusion.1 = bf16[512,2048]{1,0:T(8,128)(2,1)} fusion(bf16[1408,2048]{1,0:T(8,128)(2,1)} %bitcast.30, bf16[1408,2048]{1,0:T(8,128)(2,1)} %bitcast.32, f32[512,1408]{1,0:T(8,128)} %fusion.14, bf16[512,2048]{1,0:T(8,128)(2,1)S(1)} %copy-done, f32[512]{0:T(512)S(1)} %add_rsqrt_fusion), kind=kOutput, calls=%fused_computation.9 | convolution fusion | flops 5914099712 | bytes 18614272 | tf_op jit(solution)/shard_map/dot_general | solution.py:334
  130.7 46.7 %reduce-scatter.3.cloned.1.call-done = bf16[128,2048]{1,0:T(8,128)(2,1)} async-done(((bf16[512,2048]{1,0:T(8,128)(2,1)}), bf16[128,2048]{1,0:T(8,128)(2,1)}) %reduce-scatter.3.cloned.1.call-update) | async-done | bytes 524304 | tf_op jit(solution)/shard_map/reduce_scatter | solution.py:333
  178.7 1.5 fusion.10
  181.3 3.0 shard_map.94.refs_1_
  184.3 3.0 shard_map.93.refs_0_
  187.3 3.0 shard_map.95
  190.3 115.9 %shard_map.96 = (bf16[4,2,176,2048]{3,2,1,0:T(8,128)(2,1)}, bf16[4,2,176,2048]{3,2,1,0:T(8,128)(2,1)}, bf16[4,2,176,2048]{3,2,1,0:T(8,128)(2,1)}) custom-call(bf16[4,176,512]{2,1,0:T(8,128)(2,1)} %shard_map.93.refs_0_, bf16[4,176,512]{2,1,0:T(8,128)(2,1)} %shard_map.94.refs_1_, bf16[4,2,176,512]{3,2,1,0:T(8,128)(2,1)} %bitcast.26), custom_call_target="tpu_custom_call" | custom-call | bytes 230686720 | tf_op jit(solution)/shard_map/pallas_call | solution.py:254
  306.3 8.4 %fusion.21 = f32[512,1408]{1,0:T(8,128)} fusion(bf16[512,2048]{1,0:T(8,128)(2,1)} %all-gather.2.cloned.1.call-done, bf16[1408,2048]{1,0:T(8,128)(2,1)} %bitcast.20), kind=kOutput, calls=%fused_computation.35 | convolution fusion | flops 2952790016 | bytes 10747904 | tf_op jit(solution)/shard_map/dot_general | solution.py:330
  314.7 13.3 %convolution_convert_fusion = bf16[512,2048]{1,0:T(8,128)(2,1)} fusion(bf16[1408,2048]{1,0:T(8,128)(2,1)} %bitcast.22, bf16[512,2048]{1,0:T(8,128)(2,1)S(1)} %copy-done.2, bf16[1408,2048]{1,0:T(8,128)(2,1)} %bitcast.24, f32[512,1408]{1,0:T(8,128)} %fusion.21), kind=kOutput, calls=%fused_computation.8 | convolution fusion | flops 5910953984 | bytes 18612224 | tf_op jit(solution)/shard_map/dot_general | solution.py:334
  328.0 8.2 %shard_map.103.refs_0_ = bf16[2,2048,1408]{2,1,0:T(8,128)(2,1)} custom-call(bf16[1408,2048]{1,0:T(8,128)(2,1)} %bitcast.33), custom_call_target="tpu_custom_call" | custom-call | bytes 11534336 | tf_op jit(solution)/shard_map/pallas_call | solution.py:286
  336.2 8.3 %shard_map.105.refs_0_ = bf16[2,2048,1408]{2,1,0:T(8,128)(2,1)} custom-call(bf16[1408,2048]{1,0:T(8,128)(2,1)} %bitcast.31), custom_call_target="tpu_custom_call" | custom-call | bytes 11534336 | tf_op jit(solution)/shard_map/pallas_call | solution.py:286
  344.5 8.3 %shard_map.101.refs_0_ = bf16[2,2048,1408]{2,1,0:T(8,128)(2,1)} custom-call(bf16[1408,2048]{1,0:T(8,128)(2,1)} %bitcast.29), custom_call_target="tpu_custom_call" | custom-call | bytes 11534336 | tf_op jit(solution)/shard_map/pallas_call | solution.py:286
  352.8 8.2 %shard_map.104 = bf16[2,2048,1408]{2,1,0:T(8,128)(2,1)} custom-call(bf16[1408,2048]{1,0:T(8,128)(2,1)} %bitcast.25, bf16[2,2048,1408]{2,1,0:T(8,128)(2,1)} %shard_map.103.refs_0_), custom_call_target="tpu_custom_call", output_to_operand_aliasing={{}: (1, {})} | custom-call | bytes 11534336 | tf_op jit(solution)/shard_map/pallas_call | solution.py:286
  361.0 8.2 %shard_map.106 = bf16[2,2048,1408]{2,1,0:T(8,128)(2,1)} custom-call(bf16[1408,2048]{1,0:T(8,128)(2,1)} %bitcast.23, bf16[2,2048,1408]{2,1,0:T(8,128)(2,1)} %shard_map.105.refs_0_), custom_call_target="tpu_custom_call", output_to_operand_aliasing={{}: (1, {})} | custom-call | bytes 11534336 | tf_op jit(solution)/shard_map/pallas_call | solution.py:286
  369.2 8.2 %shard_map.102 = bf16[2,2048,1408]{2,1,0:T(8,128)(2,1)} custom-call(bf16[1408,2048]{1,0:T(8,128)(2,1)} %bitcast.21, bf16[2,2048,1408]{2,1,0:T(8,128)(2,1)} %shard_map.101.refs_0_), custom_call_target="tpu_custom_call", output_to_operand_aliasing={{}: (1, {})} | custom-call | bytes 11534336 | tf_op jit(solution)/shard_map/pallas_call | solution.py:286
  377.5 1.2 fusion.8
  378.7 2.1 fusion.12
  (21 shorter events, 2.6 us)
Async XLA Ops:
  7.2 170.3 %reduce-scatter.3.cloned.1.call-start = ((), (), s32[]{:S(2)}) async-start(), calls=%async_computation.2 | async-start | bytes 2621440 | tf_op jit(solution)/shard_map/reduce_scatter | solution.py:333
  19.9 89.7 %copy-start = (bf16[512,2048]{1,0:T(8,128)(2,1)S(1)}, bf16[512,2048]{1,0:T(8,128)(2,1)}, u32[]{:S(2)}) copy-start(bf16[512,2048]{1,0:T(8,128)(2,1)} %param.6) | copy-start | bytes 6291460
  117.3 13.4 %copy-start.1 = (f32[2,2048]{1,0:T(2,128)S(1)}, f32[2,2048]{1,0:T(2,128)}, u32[]{:S(2)}) copy-start(f32[2,2048]{1,0:T(2,128)} %param.11) | copy-start | bytes 49156
  130.6 175.6 %all-gather.2.cloned.1.call-start = ((), (), s32[]{:S(2)}) async-start(), calls=%async_computation.3 | async-start | bytes 2621440 | tf_op jit(solution)/shard_map/all_gather | solution.py:329
  181.1 196.4 %reduce-scatter.5.cloned.1.call-start = ((), (), s32[]{:S(2)}) async-start(), calls=%async_computation.4 | async-start | bytes 2621440 | tf_op jit(solution)/shard_map/reduce_scatter | solution.py:333
  306.2 8.5 %copy-start.2 = (bf16[512,2048]{1,0:T(8,128)(2,1)S(1)}, bf16[512,2048]{1,0:T(8,128)(2,1)}, u32[]{:S(2)}) copy-start(bf16[512,2048]{1,0:T(8,128)(2,1)} %all-gather.2.cloned.1.call-done) | copy-start | bytes 6291460
Sparse Core Ops, SparseCore 0:
  130.8 46.6 reduce-scatter.2
  181.2 91.9 all-gather.1
  328.1 49.2 reduce-scatter.4

commit v3 on v2

--- a/solution.py
+++ b/solution.py
@@ -83,6 +83,9 @@
     return (jnp.stack(gates), jnp.stack(ups), jnp.stack(downs), rounded_state)
 
 
+COVER = 3
+
+
 def prep_kernel(blocks, width, part, scaled, where, *refs):
     if scaled:
         gain, weight, out, flip = refs
@@ -310,35 +313,42 @@
     where = lax.axis_index("grp")[None].astype(jnp.int32)
     gain_column = in_gain[:, :, None]
     contract_last = (((1,), (1,)), ((), ()))
-    flips = []
-    for layer in range(2):
-        pieces = [
+    pieces = [
+        [
             prepare(where, gate_weight, gain_column, layer, groups, halves),
             prepare(where, up_weight, gain_column, layer, groups, halves),
             prepare(where, down_weight, None, layer, groups, 1),
         ]
-        whole = spread(pieces, layer, groups, columns)
-        flips.append([mat.reshape(columns * block_width, model_width) for mat in whole])
+        for layer in range(2)
+    ]
     residual = lax.dynamic_slice_in_dim(tokens, here * rows_mine, rows_mine, 0).astype(jnp.float32)
     normed = normalize(tokens.astype(jnp.float32)).astype(jnp.bfloat16)
     stacked = [None, None, None]
+    whole = spread(pieces[0], 0, groups, columns)
     for layer in range(2):
-        gate_flip, up_flip, down_flip = flips[layer]
-        stacked = [emit(flip, layer, held) for flip, held in zip(flips[layer], stacked)]
-        if layer:
-            normed = lax.all_gather(normed, "fs", axis=0, tiled=True)
+        flips = [mat.reshape(columns * block_width, model_width) for mat in whole]
+        gate_flip, up_flip, down_flip = flips
         gate_act = lax.dot_general(normed, gate_flip, contract_last, preferred_element_type=jnp.float32)
         up_act = lax.dot_general(normed, up_flip, contract_last, preferred_element_type=jnp.float32)
         hidden = (jax.nn.silu(gate_act) * up_act).astype(jnp.bfloat16)
-        mixed = lax.psum_scatter(
-            jnp.dot(hidden, down_flip, preferred_element_type=jnp.float32).astype(jnp.bfloat16),
-            "fs",
-            scatter_dimension=0,
-            tiled=True,
-        ).astype(jnp.float32)
+        partial = jnp.dot(hidden, down_flip, preferred_element_type=jnp.float32).astype(jnp.bfloat16)
+        if layer == 0:
+            partial, *later = lax.optimization_barrier((partial, *pieces[1]))
+            whole = spread(later, 1, groups, columns)
+        mixed = lax.psum_scatter(partial, "fs", scatter_dimension=0, tiled=True)
+        if layer == 0:
+            mixed, *whole = lax.optimization_barrier((mixed, *whole))
+        mixed = mixed.astype(jnp.float32)
         rounded_state = (residual + 0.5 * out_gain[layer] * normalize(mixed)).astype(jnp.bfloat16)
-        residual = rounded_state.astype(jnp.float32)
-        normed = normalize(residual).astype(jnp.bfloat16)
+        if layer == 0:
+            residual = rounded_state.astype(jnp.float32)
+            normed = normalize(residual).astype(jnp.bfloat16)
+            normed, *flips = lax.optimization_barrier((normed, *flips))
+            normed = lax.all_gather(normed, "fs", axis=0, tiled=True)
+            stacked = [emit(flip, 0, None) for flip in flips]
+            normed, *stacked[:COVER] = lax.optimization_barrier((normed, *stacked[:COVER]))
+        else:
+            stacked = [emit(flip, 1, held) for flip, held in zip(flips, stacked)]
     return (*stacked, rounded_state)
 
 

time: 394 us -> 392 us (level); the launches traced: 387 us -> 391 us
  Pallas kernels: 273 us -> 278 us
    reduce_scatter x2, waiting for transfers between devices: 46.7 us -> 17.8 us  [body(): mixed = lax.psum_scatter(partial, 'fs', scatter_dimension=0, tiled=True)]
    all_gather x1, waiting for transfers between devices: 0.02 us -> 28.7 us  [body(): normed = lax.all_gather(normed, 'fs', axis=0, tiled=True)]
    pallas_call x2, Pallas kernels: 206 us -> 211 us  [spread(): pl.pallas_call(functools.partial(spread_kernel, blocks), in_specs=[pl.Blo...]
  transfers between devices with their start and end apart: 3 -> 3, of which waited for: 1 -> 2; matrix products, arithmetic and copies ran while one was open for 0% -> 0% of each run, Pallas kernels for 45% -> 44%
where the time goes in v3:
time: 392 us; the launch traced here: 391 us
  Pallas kernels  278 us (71%)
  waiting for transfers between devices  46.5 us (12%)
  matrix products  42.8 us (11%)
  between operations  13.8 us (4%)
  other arithmetic  7.5 us (2%)
    pallas_call x2, Pallas kernels, spread(): pl.pallas_call(functools.partial(spread_kernel, blocks), in_specs=[pl.Blo...  211 us
    pallas_call x6, Pallas kernels, emit(): pl.pallas_call(emit_kernel, grid=(width // step,), in_specs=in_specs, out...  49.6 us
    all_gather x1, waiting for transfers between devices, body(): normed = lax.all_gather(normed, 'fs', axis=0, tiled=True)  28.7 us
    dot_general x2, matrix products, body(): jnp.dot(hidden, down_flip, preferred_element_type=jnp.float32)  26.7 us
    pallas_call x6, Pallas kernels, prepare(): pl.pallas_call(functools.partial(prep_kernel, blocks, width, part, gain i...  17.9 us
    reduce_scatter x2, waiting for transfers between devices, body(): mixed = lax.psum_scatter(partial, 'fs', scatter_dimension=0, tiled=True)  17.8 us
    dot_general x2, matrix products, body(): lax.dot_general(normed, gate_flip, contract_last, preferred_element_type=...  16.1 us
  transfers between devices with their start and end apart: 3, of which 2 were waited for; matrix products, arithmetic and copies ran while one was open for 0% of the time, Pallas kernels for 44%

profile of v3, /device:TPU:0, one launch (start us, length us, event | category | flops | bytes accessed | tf_op | source)
XLA Modules:
  0.0 390.9 jit_solution(2714225702061291940)
XLA Ops:
  7.2 1.7 copy.13.refs_0_
  8.9 3.0 shard_map.93.refs_0_
  11.9 3.0 shard_map.97.refs_0_
  14.9 3.0 shard_map.94.refs_1_
  17.9 3.0 shard_map.98.refs_1_
  20.9 2.9 shard_map.95
  23.8 3.0 shard_map.99
  27.3 89.8 %shard_map.96 = (bf16[4,2,176,2048]{3,2,1,0:T(8,128)(2,1)}, bf16[4,2,176,2048]{3,2,1,0:T(8,128)(2,1)}, bf16[4,2,176,2048]{3,2,1,0:T(8,128)(2,1)}) custom-call(bf16[4,176,512]{2,1,0:T(8,128)(2,1)} %shard_map.93.refs_0_, bf16[4,176,512]{2,1,0:T(8,128)(2,1)} %shard_map.94.refs_1_, bf16[4,2,176,512]{3,2,1,0:T(8,128)(2,1)} %bitcast.27), custom_call_target="tpu_custom_call" | custom-call | bytes 230686720 | tf_op jit(solution)/shard_map/pallas_call | solution.py:257
  117.1 7.7 %fusion.14 = f32[512,1408]{1,0:T(8,128)} fusion(bf16[1408,2048]{1,0:T(8,128)(2,1)} %bitcast.32, bf16[512,2048]{1,0:T(8,128)(2,1)S(1)} %copy-done, f32[512]{0:T(512)S(1)} %add_rsqrt_fusion), kind=kOutput, calls=%fused_computation.26 | convolution fusion | flops 2955935744 | bytes 10749952 | tf_op jit(solution)/shard_map/dot_general | solution.py:331
  124.8 13.3 %convolution_convert_fusion.1 = bf16[512,2048]{1,0:T(8,128)(2,1)} fusion(bf16[1408,2048]{1,0:T(8,128)(2,1)} %bitcast.28, bf16[1408,2048]{1,0:T(8,128)(2,1)} %bitcast.30, f32[512,1408]{1,0:T(8,128)} %fusion.14, bf16[512,2048]{1,0:T(8,128)(2,1)S(1)} %copy-done, f32[512]{0:T(512)S(1)} %add_rsqrt_fusion), kind=kOutput, calls=%fused_computation.9 | convolution fusion | flops 5914099712 | bytes 18614272 | tf_op jit(solution)/shard_map/dot_general | solution.py:334
  138.4 121.0 %shard_map.100 = (bf16[4,2,176,2048]{3,2,1,0:T(8,128)(2,1)}, bf16[4,2,176,2048]{3,2,1,0:T(8,128)(2,1)}, bf16[4,2,176,2048]{3,2,1,0:T(8,128)(2,1)}) custom-call(bf16[4,176,512]{2,1,0:T(8,128)(2,1)} %shard_map.97.refs_0_, bf16[4,176,512]{2,1,0:T(8,128)(2,1)} %shard_map.98.refs_1_, bf16[4,2,176,512]{3,2,1,0:T(8,128)(2,1)} %bitcast.26), custom_call_target="tpu_custom_call" | custom-call | bytes 230686720 | tf_op jit(solution)/shard_map/pallas_call | solution.py:257
  259.5 1.2 fusion.4
  260.7 1.5 fusion.10
  263.2 8.2 %shard_map.101.refs_0_ = bf16[2,2048,1408]{2,1,0:T(8,128)(2,1)} custom-call(bf16[1408,2048]{1,0:T(8,128)(2,1)} %bitcast.33), custom_call_target="tpu_custom_call" | custom-call | bytes 11534336 | tf_op jit(solution)/shard_map/pallas_call | solution.py:289
  271.4 8.3 %shard_map.102.refs_0_ = bf16[2,2048,1408]{2,1,0:T(8,128)(2,1)} custom-call(bf16[1408,2048]{1,0:T(8,128)(2,1)} %bitcast.31), custom_call_target="tpu_custom_call" | custom-call | bytes 11534336 | tf_op jit(solution)/shard_map/pallas_call | solution.py:289
  279.7 8.2 %shard_map.103.refs_0_ = bf16[2,2048,1408]{2,1,0:T(8,128)(2,1)} custom-call(bf16[1408,2048]{1,0:T(8,128)(2,1)} %bitcast.29), custom_call_target="tpu_custom_call" | custom-call | bytes 11534336 | tf_op jit(solution)/shard_map/pallas_call | solution.py:289
  287.9 28.7 %all-gather.2.cloned.1.call-done = bf16[512,2048]{1,0:T(8,128)(2,1)} async-done(((bf16[128,2048]{1,0:T(8,128)(2,1)}), bf16[512,2048]{1,0:T(8,128)(2,1)}) %all-gather.2.cloned.1.call-update) | async-done | bytes 2097168 | tf_op jit(solution)/shard_map/all_gather | solution.py:347
  316.6 8.4 %fusion.21 = f32[512,1408]{1,0:T(8,128)} fusion(bf16[512,2048]{1,0:T(8,128)(2,1)} %all-gather.2.cloned.1.call-done, bf16[1408,2048]{1,0:T(8,128)(2,1)} %bitcast.20), kind=kOutput, calls=%fused_computation.35 | convolution fusion | flops 2952790016 | bytes 10747904 | tf_op jit(solution)/shard_map/dot_general | solution.py:331
  325.1 13.4 %convolution_convert_fusion = bf16[512,2048]{1,0:T(8,128)(2,1)} fusion(bf16[1408,2048]{1,0:T(8,128)(2,1)} %bitcast.24, bf16[512,2048]{1,0:T(8,128)(2,1)S(1)} %copy-done.2, bf16[1408,2048]{1,0:T(8,128)(2,1)} %bitcast.22, f32[512,1408]{1,0:T(8,128)} %fusion.21), kind=kOutput, calls=%fused_computation.8 | convolution fusion | flops 5910953984 | bytes 18612224 | tf_op jit(solution)/shard_map/dot_general | solution.py:334
  338.4 8.2 %shard_map.106 = bf16[2,2048,1408]{2,1,0:T(8,128)(2,1)} custom-call(bf16[1408,2048]{1,0:T(8,128)(2,1)} %bitcast.25, bf16[2,2048,1408]{2,1,0:T(8,128)(2,1)} %shard_map.103.refs_0_), custom_call_target="tpu_custom_call", output_to_operand_aliasing={{}: (1, {})} | custom-call | bytes 11534336 | tf_op jit(solution)/shard_map/pallas_call | solution.py:289
  346.7 8.3 %shard_map.105 = bf16[2,2048,1408]{2,1,0:T(8,128)(2,1)} custom-call(bf16[1408,2048]{1,0:T(8,128)(2,1)} %bitcast.23, bf16[2,2048,1408]{2,1,0:T(8,128)(2,1)} %shard_map.102.refs_0_), custom_call_target="tpu_custom_call", output_to_operand_aliasing={{}: (1, {})} | custom-call | bytes 11534336 | tf_op jit(solution)/shard_map/pallas_call | solution.py:289
  355.0 8.3 %shard_map.104 = bf16[2,2048,1408]{2,1,0:T(8,128)(2,1)} custom-call(bf16[1408,2048]{1,0:T(8,128)(2,1)} %bitcast.21, bf16[2,2048,1408]{2,1,0:T(8,128)(2,1)} %shard_map.101.refs_0_), custom_call_target="tpu_custom_call", output_to_operand_aliasing={{}: (1, {})} | custom-call | bytes 11534336 | tf_op jit(solution)/shard_map/pallas_call | solution.py:289
  363.2 17.8 %reduce-scatter.5.cloned.1.call-done = bf16[128,2048]{1,0:T(8,128)(2,1)} async-done(((bf16[512,2048]{1,0:T(8,128)(2,1)}), bf16[128,2048]{1,0:T(8,128)(2,1)}) %reduce-scatter.5.cloned.1.call-update) | async-done | bytes 524304 | tf_op jit(solution)/shard_map/reduce_scatter | solution.py:338
  382.3 2.1 fusion.12
  (21 shorter events, 3.1 us)
Async XLA Ops:
  7.2 252.3 %reduce-scatter.3.cloned.1.call-start = ((), (), s32[]{:S(2)}) async-start(), calls=%async_computation.2 | async-start | bytes 2621440 | tf_op jit(solution)/shard_map/reduce_scatter | solution.py:338
  23.8 3.0 copy-start
  138.1 121.3 %copy-start.1 = (f32[2,2048]{1,0:T(2,128)S(1)}, f32[2,2048]{1,0:T(2,128)}, u32[]{:S(2)}) copy-start(f32[2,2048]{1,0:T(2,128)} %param.11) | copy-start | bytes 49156
  138.1 178.5 %all-gather.2.cloned.1.call-start = ((), (), s32[]{:S(2)}) async-start(), calls=%async_computation.3 | async-start | bytes 2621440 | tf_op jit(solution)/shard_map/all_gather | solution.py:347
  263.1 117.9 %reduce-scatter.5.cloned.1.call-start = ((), (), s32[]{:S(2)}) async-start(), calls=%async_computation.4 | async-start | bytes 2621440 | tf_op jit(solution)/shard_map/reduce_scatter | solution.py:338
  316.6 8.4 %copy-start.2 = (bf16[512,2048]{1,0:T(8,128)(2,1)S(1)}, bf16[512,2048]{1,0:T(8,128)(2,1)}, u32[]{:S(2)}) copy-start(bf16[512,2048]{1,0:T(8,128)(2,1)} %all-gather.2.cloned.1.call-done) | copy-start | bytes 6291460
Sparse Core Ops, SparseCore 0:
  138.3 81.5 reduce-scatter.2
  263.3 53.3 all-gather.1
  338.6 42.4 reduce-scatter.4

commit v4 on v3

--- a/solution.py
+++ b/solution.py
@@ -83,9 +83,6 @@
     return (jnp.stack(gates), jnp.stack(ups), jnp.stack(downs), rounded_state)
 
 
-COVER = 3
-
-
 def prep_kernel(blocks, width, part, scaled, where, *refs):
     if scaled:
         gain, weight, out, flip = refs
@@ -126,9 +123,10 @@
     )(where, *args)
 
 
-def spread_kernel(blocks, *refs):
-    sources, full = refs[:3], refs[3:6]
-    own, (own_sem, send_sem, recv_sem) = refs[6:9], refs[9:]
+def spread_kernel(blocks, split, *refs):
+    n = len(split)
+    sources, full = refs[:n], refs[n : 2 * n]
+    own, (own_sem, send_sem, recv_sem) = refs[2 * n : 3 * n], refs[3 * n :]
     y, z, t = lax.axis_index("grp"), lax.axis_index("fs"), lax.axis_index("tp")
     x, c = t // 2, lax.rem(t, 2)
     other_y, other_x, other_c = 1 - y, (1 - x) * 2 + c, x * 2 + (1 - c)
@@ -146,12 +144,12 @@
 
     def place(m, column, half, source):
         cols = columns(source)
-        if m == 2:
+        if not split[m]:
             return full[m].at[column, :, :, cols]
         return full[m].at[column, half, :, cols]
 
     def rows_of(m, column, half):
-        if m == 2:
+        if not split[m]:
             return full[m].at[column]
         return full[m].at[column, half]
 
@@ -192,45 +190,47 @@
 
     to_x, to_c, to_y = {"tp": other_x}, {"tp": other_c}, {"grp": other_y}
     fetch = []
-    for m in range(3):
+    for m in range(n):
         for shift in range(1, blocks):
             target = lax.rem(z + shift, blocks)
             send(("z", m, shift), origin(m, target), place(m, t, y, z), {"fs": target})
         mine = origin(m, z)
         send(("x", m, 0), mine, place(m, t, y, z), to_x)
-        if m < 2:
+        if split[m]:
             send(("y", m, 0, 0), mine, place(m, t, y, z), to_y)
         copy = pltpu.make_async_copy(mine, own[m], own_sem.at[m])
         copy.start()
         fetch.append(copy)
     kept = []
-    for m in range(3):
+    for m in range(n):
         fetch[m].wait()
-        copy = pltpu.make_async_copy(own[m], place(m, t, y, z), own_sem.at[3 + m])
+        copy = pltpu.make_async_copy(own[m], place(m, t, y, z), own_sem.at[n + m])
         copy.start()
         kept.append(copy)
 
     def relay(m, shift):
         source = lax.rem(z + blocks - shift, blocks)
         arrived(("x", m, shift), place(m, other_x, y, source), to_x)
-        if m < 2:
+        if split[m]:
             spot = place(m, other_x, y, source)
             send(("y", m, 1, shift), spot, spot, to_y)
 
-    for m in range(3):
+    for m in range(n):
         for shift in range(1, blocks):
             source = lax.rem(z + blocks - shift, blocks)
             spot = place(m, t, y, source)
             arrived(("z", m, shift), spot, {"fs": source})
             send(("x", m, shift), spot, spot, to_x)
-            if m < 2:
+            if split[m]:
                 send(("y", m, 0, shift), spot, spot, to_y)
             relay(m, shift - 1)
         kept[m].wait()
         send(("c", m, 0, 0), rows_of(m, t, y), rows_of(m, t, y), to_c)
         relay(m, blocks - 1)
         send(("c", m, 1, 0), rows_of(m, other_x, y), rows_of(m, other_x, y), to_c)
-    for m in range(2):
+    for m in range(n):
+        if not split[m]:
+            continue
         for far, column in ((0, t), (1, other_x)):
             for shift in range(blocks):
                 source = lax.rem(z + blocks - shift, blocks)
@@ -238,37 +238,39 @@
             rows = rows_of(m, column, other_y)
             send(("c", m, far, 1), rows, rows, to_c)
     other_both = (1 - x) * 2 + (1 - c)
-    for m in range(3):
+    for m in range(n):
         for far, column in ((0, other_c), (1, other_both)):
             arrived(("c", m, far, 0), rows_of(m, column, y), to_c)
-            if m < 2:
+            if split[m]:
                 arrived(("c", m, far, 1), rows_of(m, column, other_y), to_c)
     for copy in sent:
         copy.wait_send()
 
 
-def spread(sources, layer, blocks, columns):
-    halves, part = 2, sources[0].shape[1]
-    rows = sources[0].shape[2]
-    sources = [sources[0], sources[1], sources[2].reshape(blocks, halves, part, rows)]
-    count = 3 * (blocks - 1) + 3 * blocks + 4 * blocks + 10
+def spread(sources, split, blocks, columns):
+    n, halves = len(split), 2
+    part, rows = sources[0].shape[1:]
+    sources = [
+        source if alone else source.reshape(blocks, halves, part, rows)
+        for source, alone in zip(sources, split)
+    ]
+    count = sum(4 * blocks + 1 + (2 * blocks + 2) * alone for alone in split)
     shape = (columns, halves, part, rows * blocks)
-    moved = columns * halves * part * rows * blocks * 2
+    moved = n * columns * halves * part * rows * blocks * 2
+    whole = pl.BlockSpec(memory_space=pl.ANY)
     return pl.pallas_call(
-        functools.partial(spread_kernel, blocks),
-        in_specs=[pl.BlockSpec(memory_space=pl.ANY)] * 3,
-        out_specs=[pl.BlockSpec(memory_space=pl.ANY)] * 3,
-        out_shape=[jax.ShapeDtypeStruct(shape, jnp.bfloat16)] * 3,
-        scratch_shapes=[
-            pltpu.VMEM((part, rows), jnp.bfloat16),
-            pltpu.VMEM((part, rows), jnp.bfloat16),
-            pltpu.VMEM((halves, part, rows), jnp.bfloat16),
-            pltpu.SemaphoreType.DMA((6,)),
+        functools.partial(spread_kernel, blocks, split),
+        in_specs=[whole] * n,
+        out_specs=[whole] * n,
+        out_shape=[jax.ShapeDtypeStruct(shape, jnp.bfloat16)] * n,
+        scratch_shapes=[pltpu.VMEM(source.shape[1:], jnp.bfloat16) for source in sources]
+        + [
+            pltpu.SemaphoreType.DMA((2 * n,)),
             pltpu.SemaphoreType.DMA((count,)),
             pltpu.SemaphoreType.DMA((count,)),
         ],
-        compiler_params=pltpu.CompilerParams(collective_id=layer, has_side_effects=True),
-        cost_estimate=pl.CostEstimate(flops=0, bytes_accessed=moved * 40, transcendentals=0),
+        compiler_params=pltpu.CompilerParams(collective_id=0, has_side_effects=True),
+        cost_estimate=pl.CostEstimate(flops=0, bytes_accessed=moved * 13, transcendentals=0),
     )(*sources)
 
 
@@ -323,32 +325,36 @@
     ]
     residual = lax.dynamic_slice_in_dim(tokens, here * rows_mine, rows_mine, 0).astype(jnp.float32)
     normed = normalize(tokens.astype(jnp.float32)).astype(jnp.bfloat16)
-    stacked = [None, None, None]
-    whole = spread(pieces[0], 0, groups, columns)
+    order = ((0, 0), (0, 1), (1, 0), (1, 1), (0, 2), (1, 2))
+    split = tuple(which < 2 for _, which in order)
+    sent = [pieces[layer][which] for layer, which in order]
+    whole = dict(zip(order, spread(sent, split, groups, columns)))
+    sampler = [
+        [whole[layer, which].reshape(columns * block_width, model_width) for which in range(3)]
+        for layer in range(2)
+    ]
     for layer in range(2):
-        flips = [mat.reshape(columns * block_width, model_width) for mat in whole]
+        flips = sampler[layer]
         gate_flip, up_flip, down_flip = flips
         gate_act = lax.dot_general(normed, gate_flip, contract_last, preferred_element_type=jnp.float32)
         up_act = lax.dot_general(normed, up_flip, contract_last, preferred_element_type=jnp.float32)
         hidden = (jax.nn.silu(gate_act) * up_act).astype(jnp.bfloat16)
         partial = jnp.dot(hidden, down_flip, preferred_element_type=jnp.float32).astype(jnp.bfloat16)
-        if layer == 0:
-            partial, *later = lax.optimization_barrier((partial, *pieces[1]))
-            whole = spread(later, 1, groups, columns)
         mixed = lax.psum_scatter(partial, "fs", scatter_dimension=0, tiled=True)
         if layer == 0:
-            mixed, *whole = lax.optimization_barrier((mixed, *whole))
+            mixed, first = lax.optimization_barrier((mixed, [emit(flip, 0, None) for flip in flips]))
         mixed = mixed.astype(jnp.float32)
         rounded_state = (residual + 0.5 * out_gain[layer] * normalize(mixed)).astype(jnp.bfloat16)
         if layer == 0:
             residual = rounded_state.astype(jnp.float32)
             normed = normalize(residual).astype(jnp.bfloat16)
-            normed, *flips = lax.optimization_barrier((normed, *flips))
+            normed, first = lax.optimization_barrier((normed, first))
             normed = lax.all_gather(normed, "fs", axis=0, tiled=True)
-            stacked = [emit(flip, 0, None) for flip in flips]
-            normed, *stacked[:COVER] = lax.optimization_barrier((normed, *stacked[:COVER]))
+            early = emit(sampler[1][0], 1, first[0])
+            normed, early = lax.optimization_barrier((normed, early))
+            stacked = [early, *first[1:]]
         else:
-            stacked = [emit(flip, 1, held) for flip, held in zip(flips, stacked)]
+            stacked[1:] = [emit(flip, 1, held) for flip, held in zip(flips[1:], stacked[1:])]
     return (*stacked, rounded_state)
 
 

time: 392 us -> 385 us (0.982)
  Pallas kernels: 278 us -> 233 us
  waiting for transfers between devices: 46.5 us -> 84.5 us
    pallas_call x2 -> x1, Pallas kernels: 211 us -> 165 us  [spread(): pl.pallas_call(functools.partial(spread_kernel, blocks, split), in_specs=...]
    reduce_scatter x2, waiting for transfers between devices: 17.8 us -> 47.8 us  [body(): mixed = lax.psum_scatter(partial, 'fs', scatter_dimension=0, tiled=True)]
    all_gather x1, waiting for transfers between devices: 28.7 us -> 36.6 us  [body(): normed = lax.all_gather(normed, 'fs', axis=0, tiled=True)]
  transfers between devices with their start and end apart: 3 -> 3, of which waited for: 2 -> 3; matrix products, arithmetic and copies ran while one was open for 0% -> 0% of each run, Pallas kernels for 44% -> 13%
where the time goes in v4:
time: 385 us; the launch traced here: 384 us
  Pallas kernels  233 us (61%)
  waiting for transfers between devices  84.5 us (22%)
  matrix products  42.8 us (11%)
  between operations  13.8 us (4%)
  other arithmetic  7.5 us (2%)
    pallas_call x1, Pallas kernels, spread(): pl.pallas_call(functools.partial(spread_kernel, blocks, split), in_specs=...  165 us
    pallas_call x6, Pallas kernels, emit(): pl.pallas_call(emit_kernel, grid=(width // step,), in_specs=in_specs, out...  49.8 us
    reduce_scatter x2, waiting for transfers between devices, body(): mixed = lax.psum_scatter(partial, 'fs', scatter_dimension=0, tiled=True)  47.8 us
    all_gather x1, waiting for transfers between devices, body(): normed = lax.all_gather(normed, 'fs', axis=0, tiled=True)  36.6 us
    dot_general x2, matrix products, body(): jnp.dot(hidden, down_flip, preferred_element_type=jnp.float32)  26.7 us
    pallas_call x6, Pallas kernels, prepare(): pl.pallas_call(functools.partial(prep_kernel, blocks, width, part, gain i...  18 us
    dot_general x2, matrix products, body(): lax.dot_general(normed, gate_flip, contract_last, preferred_element_type=...  16.1 us
  transfers between devices with their start and end apart: 3, of which 3 were waited for; matrix products, arithmetic and copies ran while one was open for 0% of the time, Pallas kernels for 13%

profile of v4, /device:TPU:0, one launch (start us, length us, event | category | flops | bytes accessed | tf_op | source)
XLA Modules:
  0.0 383.6 jit_solution(9476571032807753940)
XLA Ops:
  7.2 1.7 copy.13.refs_0_
  8.9 3.0 shard_map.93.refs_0_
  11.9 3.0 shard_map.95.refs_2_
  14.9 3.0 shard_map.94.refs_1_
  17.9 3.0 shard_map.96.refs_3_
  20.9 2.9 shard_map.97
  23.8 3.0 shard_map.98
  27.4 165.2 %shard_map.99 = (bf16[4,2,176,2048]{3,2,1,0:T(8,128)(2,1)}, bf16[4,2,176,2048]{3,2,1,0:T(8,128)(2,1)}, bf16[4,2,176,2048]{3,2,1,0:T(8,128)(2,1)}, bf16[4,2,176,2...) custom-call(bf16[4,176,512]{2,1,0:T(8,128)(2,1)} %shard_map.93.refs_0_, ...), custom_call_target="tpu_custom_call" | custom-call | bytes 449839104 | tf_op jit(solution)/shard_map/pallas_call | solution.py:261
  192.6 7.7 %fusion.14 = f32[512,1408]{1,0:T(8,128)} fusion(bf16[1408,2048]{1,0:T(8,128)(2,1)} %bitcast.30, bf16[512,2048]{1,0:T(8,128)(2,1)S(1)} %copy-done, f32[512]{0:T(512)S(1)} %add_rsqrt_fusion), kind=kOutput, calls=%fused_computation.26 | convolution fusion | flops 2955935744 | bytes 10749952 | tf_op jit(solution)/shard_map/dot_general | solution.py:339
  200.2 13.3 %convolution_convert_fusion.1 = bf16[512,2048]{1,0:T(8,128)(2,1)} fusion(bf16[1408,2048]{1,0:T(8,128)(2,1)} %bitcast.26, bf16[1408,2048]{1,0:T(8,128)(2,1)} %bitcast.28, f32[512,1408]{1,0:T(8,128)} %fusion.14, bf16[512,2048]{1,0:T(8,128)(2,1)S(1)} %copy-done, f32[512]{0:T(512)S(1)} %add_rsqrt_fusion), kind=kOutput, calls=%fused_computation.9 | convolution fusion | flops 5914099712 | bytes 18614272 | tf_op jit(solution)/shard_map/dot_general | solution.py:342
  213.8 8.2 %shard_map.100.refs_0_ = bf16[2,2048,1408]{2,1,0:T(8,128)(2,1)} custom-call(bf16[1408,2048]{1,0:T(8,128)(2,1)} %bitcast.31), custom_call_target="tpu_custom_call" | custom-call | bytes 11534336 | tf_op jit(solution)/shard_map/pallas_call | solution.py:291
  222.1 8.4 %shard_map.101.refs_0_ = bf16[2,2048,1408]{2,1,0:T(8,128)(2,1)} custom-call(bf16[1408,2048]{1,0:T(8,128)(2,1)} %bitcast.29), custom_call_target="tpu_custom_call" | custom-call | bytes 11534336 | tf_op jit(solution)/shard_map/pallas_call | solution.py:291
  230.5 8.3 %shard_map.102.refs_0_ = bf16[2,2048,1408]{2,1,0:T(8,128)(2,1)} custom-call(bf16[1408,2048]{1,0:T(8,128)(2,1)} %bitcast.27), custom_call_target="tpu_custom_call" | custom-call | bytes 11534336 | tf_op jit(solution)/shard_map/pallas_call | solution.py:291
  238.8 21.8 %reduce-scatter.3.cloned.1.call-done = bf16[128,2048]{1,0:T(8,128)(2,1)} async-done(((bf16[512,2048]{1,0:T(8,128)(2,1)}), bf16[128,2048]{1,0:T(8,128)(2,1)}) %reduce-scatter.3.cloned.1.call-update) | async-done | bytes 524304 | tf_op jit(solution)/shard_map/reduce_scatter | solution.py:343
  260.6 1.2 fusion.4
  261.8 1.5 fusion.10
  264.3 8.3 %shard_map.103 = bf16[2,2048,1408]{2,1,0:T(8,128)(2,1)} custom-call(bf16[1408,2048]{1,0:T(8,128)(2,1)} %bitcast.24, bf16[2,2048,1408]{2,1,0:T(8,128)(2,1)} %shard_map.100.refs_0_), custom_call_target="tpu_custom_call", output_to_operand_aliasing={{}: (1, {})} | custom-call | bytes 11534336 | tf_op jit(solution)/shard_map/pallas_call | solution.py:291
  272.6 36.6 %all-gather.2.cloned.1.call-done = bf16[512,2048]{1,0:T(8,128)(2,1)} async-done(((bf16[128,2048]{1,0:T(8,128)(2,1)}), bf16[512,2048]{1,0:T(8,128)(2,1)}) %all-gather.2.cloned.1.call-update) | async-done | bytes 2097168 | tf_op jit(solution)/shard_map/all_gather | solution.py:352
  309.2 8.4 %fusion.21 = f32[512,1408]{1,0:T(8,128)} fusion(bf16[512,2048]{1,0:T(8,128)(2,1)} %all-gather.2.cloned.1.call-done, bf16[1408,2048]{1,0:T(8,128)(2,1)} %bitcast.25), kind=kOutput, calls=%fused_computation.35 | convolution fusion | flops 2952790016 | bytes 10747904 | tf_op jit(solution)/shard_map/dot_general | solution.py:339
  317.7 13.4 %convolution_convert_fusion = bf16[512,2048]{1,0:T(8,128)(2,1)} fusion(bf16[1408,2048]{1,0:T(8,128)(2,1)} %bitcast.22, bf16[512,2048]{1,0:T(8,128)(2,1)S(1)} %copy-done.2, bf16[1408,2048]{1,0:T(8,128)(2,1)} %bitcast.20, f32[512,1408]{1,0:T(8,128)} %fusion.21), kind=kOutput, calls=%fused_computation.8 | convolution fusion | flops 5910953984 | bytes 18612224 | tf_op jit(solution)/shard_map/dot_general | solution.py:342
  331.1 8.3 %shard_map.105 = bf16[2,2048,1408]{2,1,0:T(8,128)(2,1)} custom-call(bf16[1408,2048]{1,0:T(8,128)(2,1)} %bitcast.23, bf16[2,2048,1408]{2,1,0:T(8,128)(2,1)} %shard_map.102.refs_0_), custom_call_target="tpu_custom_call", output_to_operand_aliasing={{}: (1, {})} | custom-call | bytes 11534336 | tf_op jit(solution)/shard_map/pallas_call | solution.py:291
  339.4 8.3 %shard_map.104 = bf16[2,2048,1408]{2,1,0:T(8,128)(2,1)} custom-call(bf16[1408,2048]{1,0:T(8,128)(2,1)} %bitcast.21, bf16[2,2048,1408]{2,1,0:T(8,128)(2,1)} %shard_map.101.refs_0_), custom_call_target="tpu_custom_call", output_to_operand_aliasing={{}: (1, {})} | custom-call | bytes 11534336 | tf_op jit(solution)/shard_map/pallas_call | solution.py:291
  347.6 26.0 %reduce-scatter.5.cloned.1.call-done = bf16[128,2048]{1,0:T(8,128)(2,1)} async-done(((bf16[512,2048]{1,0:T(8,128)(2,1)}), bf16[128,2048]{1,0:T(8,128)(2,1)}) %reduce-scatter.5.cloned.1.call-update) | async-done | bytes 524304 | tf_op jit(solution)/shard_map/reduce_scatter | solution.py:343
  374.9 2.1 fusion.12
  (20 shorter events, 3.1 us)
Async XLA Ops:
  7.2 253.4 %reduce-scatter.3.cloned.1.call-start = ((), (), s32[]{:S(2)}) async-start(), calls=%async_computation.2 | async-start | bytes 2621440 | tf_op jit(solution)/shard_map/reduce_scatter | solution.py:343
  23.8 3.0 copy-start
  213.6 95.7 %all-gather.2.cloned.1.call-start = ((), (), s32[]{:S(2)}) async-start(), calls=%async_computation.3 | async-start | bytes 2621440 | tf_op jit(solution)/shard_map/all_gather | solution.py:352
  230.5 8.3 %copy-start.1 = (f32[2,2048]{1,0:T(2,128)S(1)}, f32[2,2048]{1,0:T(2,128)}, u32[]{:S(2)}) copy-start(f32[2,2048]{1,0:T(2,128)} %param.11) | copy-start | bytes 49156
  264.2 109.4 %reduce-scatter.5.cloned.1.call-start = ((), (), s32[]{:S(2)}) async-start(), calls=%async_computation.4 | async-start | bytes 2621440 | tf_op jit(solution)/shard_map/reduce_scatter | solution.py:343
  309.2 8.4 %copy-start.2 = (bf16[512,2048]{1,0:T(8,128)(2,1)S(1)}, bf16[512,2048]{1,0:T(8,128)(2,1)}, u32[]{:S(2)}) copy-start(bf16[512,2048]{1,0:T(8,128)(2,1)} %all-gather.2.cloned.1.call-done) | copy-start | bytes 6291460
Sparse Core Ops, SparseCore 0:
  213.7 46.8 reduce-scatter.2
  264.4 44.8 all-gather.1
  331.2 42.4 reduce-scatter.4

commit v5 on v4

--- a/solution.py
+++ b/solution.py
@@ -323,8 +323,6 @@
         ]
         for layer in range(2)
     ]
-    residual = lax.dynamic_slice_in_dim(tokens, here * rows_mine, rows_mine, 0).astype(jnp.float32)
-    normed = normalize(tokens.astype(jnp.float32)).astype(jnp.bfloat16)
     order = ((0, 0), (0, 1), (1, 0), (1, 1), (0, 2), (1, 2))
     split = tuple(which < 2 for _, which in order)
     sent = [pieces[layer][which] for layer, which in order]
@@ -333,28 +331,31 @@
         [whole[layer, which].reshape(columns * block_width, model_width) for which in range(3)]
         for layer in range(2)
     ]
-    for layer in range(2):
-        flips = sampler[layer]
-        gate_flip, up_flip, down_flip = flips
+    def advance(layer, normed, residual):
+        gate_flip, up_flip, down_flip = sampler[layer]
         gate_act = lax.dot_general(normed, gate_flip, contract_last, preferred_element_type=jnp.float32)
         up_act = lax.dot_general(normed, up_flip, contract_last, preferred_element_type=jnp.float32)
         hidden = (jax.nn.silu(gate_act) * up_act).astype(jnp.bfloat16)
         partial = jnp.dot(hidden, down_flip, preferred_element_type=jnp.float32).astype(jnp.bfloat16)
-        mixed = lax.psum_scatter(partial, "fs", scatter_dimension=0, tiled=True)
-        if layer == 0:
-            mixed, first = lax.optimization_barrier((mixed, [emit(flip, 0, None) for flip in flips]))
-        mixed = mixed.astype(jnp.float32)
-        rounded_state = (residual + 0.5 * out_gain[layer] * normalize(mixed)).astype(jnp.bfloat16)
-        if layer == 0:
-            residual = rounded_state.astype(jnp.float32)
-            normed = normalize(residual).astype(jnp.bfloat16)
-            normed, first = lax.optimization_barrier((normed, first))
-            normed = lax.all_gather(normed, "fs", axis=0, tiled=True)
-            early = emit(sampler[1][0], 1, first[0])
-            normed, early = lax.optimization_barrier((normed, early))
-            stacked = [early, *first[1:]]
-        else:
-            stacked[1:] = [emit(flip, 1, held) for flip, held in zip(flips[1:], stacked[1:])]
+        mixed = lax.psum_scatter(partial, "fs", scatter_dimension=0, tiled=True).astype(jnp.float32)
+        return (residual + 0.5 * out_gain[layer] * normalize(mixed)).astype(jnp.bfloat16)
+
+    folded = tokens.reshape(groups, 2, rows_mine // 2, model_width)
+    states = []
+    for side in range(2):
+        rows = folded[:, side].reshape(groups * rows_mine // 2, model_width)
+        kept = lax.dynamic_index_in_dim(folded[:, side], here, 0, keepdims=False)
+        normed = normalize(rows.astype(jnp.float32)).astype(jnp.bfloat16)
+        states.append(advance(0, normed, kept.astype(jnp.float32)))
+    stacked = [emit(flip, 0, None) for flip in sampler[0]]
+    states[1], stacked[:2] = lax.optimization_barrier((states[1], stacked[:2]))
+    ends = []
+    for state in states:
+        residual = state.astype(jnp.float32)
+        normed = lax.all_gather(normalize(residual).astype(jnp.bfloat16), "fs", axis=0, tiled=True)
+        ends.append(advance(1, normed, residual))
+    stacked = [emit(flip, 1, held) for flip, held in zip(sampler[1], stacked)]
+    rounded_state = jnp.concatenate(ends)
     return (*stacked, rounded_state)
 
 

time: 385 us -> 396 us (1.029)
  matrix products: 42.8 us -> 58.4 us
  waiting for transfers between devices: 84.5 us -> 74.2 us
  other arithmetic: 7.5 us -> 11.7 us
    dot_general x4 -> x8, matrix products: 42.8 us -> 58.4 us  [the longest x4 37.3 us: advance(): jnp.dot(hidden, down_flip, preferred_element_type=jnp.float32)]
    reduce_scatter x2 -> x4, waiting for transfers between devices: 47.8 us -> 33.3 us  [advance(): lax.psum_scatter(partial, 'fs', scatter_dimension=0, tiled=True)]
    all_gather x1 -> x2, waiting for transfers between devices: 36.6 us -> 40.8 us  [body(): lax.all_gather(normalize(residual).astype(jnp.bfloat16), 'fs', axis=0, ti...]
  transfers between devices with their start and end apart: 3 -> 6, of which waited for: 3 -> 4; matrix products, arithmetic and copies ran while one was open for 0% -> 12% of each run, Pallas kernels for 13% -> 13%
where the time goes in v5:
time: 396 us; the launch traced here: 395 us
  Pallas kernels  233 us (59%)
  waiting for transfers between devices  74.2 us (19%)
  matrix products  58.4 us (15%)
  between operations  14.2 us (4%)
  other arithmetic  11.7 us (3%)
    pallas_call x1, Pallas kernels, spread(): pl.pallas_call(functools.partial(spread_kernel, blocks, split), in_specs=...  165 us
    pallas_call x6, Pallas kernels, emit(): pl.pallas_call(emit_kernel, grid=(width // step,), in_specs=in_specs, out...  49.5 us
    all_gather x2, waiting for transfers between devices, body(): lax.all_gather(normalize(residual).astype(jnp.bfloat16), 'fs', axis=0, ti...  40.8 us
    dot_general x4, matrix products, advance(): jnp.dot(hidden, down_flip, preferred_element_type=jnp.float32)  37.3 us
    reduce_scatter x4, waiting for transfers between devices, advance(): lax.psum_scatter(partial, 'fs', scatter_dimension=0, tiled=True)  33.3 us
    dot_general x4, matrix products, advance(): lax.dot_general(normed, gate_flip, contract_last, preferred_element_type=...  21.2 us
    pallas_call x6, Pallas kernels, prepare(): pl.pallas_call(functools.partial(prep_kernel, blocks, width, part, gain i...  18 us
  transfers between devices with their start and end apart: 6, of which 4 were waited for; matrix products, arithmetic and copies ran while one was open for 12% of the time, Pallas kernels for 13%

profile of v5, /device:TPU:0, one launch (start us, length us, event | category | flops | bytes accessed | tf_op | source)
XLA Modules:
  0.0 394.8 jit_solution(1291602766330586518)
XLA Ops:
  8.9 3.0 shard_map.93.refs_0_
  11.9 3.0 shard_map.95.refs_2_
  14.9 3.0 shard_map.94.refs_1_
  18.0 3.0 shard_map.96.refs_3_
  23.9 3.0 shard_map.98
  28.7 165.1 %shard_map.99 = (bf16[4,2,176,2048]{3,2,1,0:T(8,128)(2,1)}, bf16[4,2,176,2048]{3,2,1,0:T(8,128)(2,1)}, bf16[4,2,176,2048]{3,2,1,0:T(8,128)(2,1)}, bf16[4,2,176,2...) custom-call(bf16[4,176,512]{2,1,0:T(8,128)(2,1)} %shard_map.93.refs_0_, ...), custom_call_target="tpu_custom_call" | custom-call | bytes 449839104 | tf_op jit(solution)/shard_map/pallas_call | solution.py:261
  193.8 5.9 %fusion.32 = f32[256,1408]{1,0:T(8,128)} fusion(bf16[256,2048]{1,0:T(8,128)(2,1)} %bitcast.67, bf16[1408,2048]{1,0:T(8,128)(2,1)} %bitcast.60), kind=kOutput, calls=%fused_computation.68 | convolution fusion | flops 1476395008 | bytes 8257536 | tf_op jit(solution)/shard_map/dot_general | solution.py:336
  199.7 9.7 %convolution_convert_fusion.3 = bf16[256,2048]{1,0:T(8,128)(2,1)} fusion(bf16[1408,2048]{1,0:T(8,128)(2,1)} %bitcast.54, bf16[256,2048]{1,0:T(8,128)(2,1)} %bitcast.68, bf16[1408,2048]{1,0:T(8,128)(2,1)} %bitcast.57, f32[256,1408]{1,0:T(8,128)} %fusion.32), kind=kOutput, calls=%fused_computation.15 | convolution fusion | flops 2955476992 | bytes 15073280 | tf_op jit(solution)/shard_map/dot_general | solution.py:339
  209.6 5.6 %fusion.33 = f32[256,1408]{1,0:T(8,128)} fusion(bf16[256,2048]{1,0:T(8,128)(2,1)S(1)} %bitcast.65, bf16[1408,2048]{1,0:T(8,128)(2,1)} %bitcast.61), kind=kOutput, calls=%fused_computation.69 | convolution fusion | flops 1476395008 | bytes 8257536 | tf_op jit(solution)/shard_map/dot_general | solution.py:336
  215.2 9.5 %convolution_convert_fusion.2 = bf16[256,2048]{1,0:T(8,128)(2,1)} fusion(bf16[1408,2048]{1,0:T(8,128)(2,1)} %bitcast.55, bf16[256,2048]{1,0:T(8,128)(2,1)S(1)} %bitcast.66, bf16[1408,2048]{1,0:T(8,128)(2,1)} %bitcast.58, f32[256,1408]{1,0:T(8,128)} %fusion.33), kind=kOutput, calls=%fused_computation.14 | convolution fusion | flops 2955476992 | bytes 15073280 | tf_op jit(solution)/shard_map/dot_general | solution.py:339
  224.7 8.3 %shard_map.100.refs_0_ = bf16[2,2048,1408]{2,1,0:T(8,128)(2,1)} custom-call(bf16[1408,2048]{1,0:T(8,128)(2,1)} %bitcast.62), custom_call_target="tpu_custom_call" | custom-call | bytes 11534336 | tf_op jit(solution)/shard_map/pallas_call | solution.py:291
  233.0 8.3 %shard_map.101.refs_0_ = bf16[2,2048,1408]{2,1,0:T(8,128)(2,1)} custom-call(bf16[1408,2048]{1,0:T(8,128)(2,1)} %bitcast.59), custom_call_target="tpu_custom_call" | custom-call | bytes 11534336 | tf_op jit(solution)/shard_map/pallas_call | solution.py:291
  243.6 24.6 %reduce-scatter.7.cloned.1.call-done = bf16[64,2048]{1,0:T(8,128)(2,1)} async-done(((bf16[256,2048]{1,0:T(8,128)(2,1)}), bf16[64,2048]{1,0:T(8,128)(2,1)}) %reduce-scatter.7.cloned.1.call-update) | async-done | bytes 262160 | tf_op jit(solution)/shard_map/reduce_scatter | solution.py:340
  272.8 25.7 %all-gather.5.cloned.1.call-done = bf16[256,2048]{1,0:T(8,128)(2,1)} async-done(((bf16[64,2048]{1,0:T(8,128)(2,1)}), bf16[256,2048]{1,0:T(8,128)(2,1)}) %all-gather.5.cloned.1.call-update) | async-done | bytes 1048592 | tf_op jit(solution)/shard_map/all_gather | solution.py:355
  298.5 4.9 %fusion.35 = f32[256,1408]{1,0:T(8,128)S(1)} fusion(bf16[256,2048]{1,0:T(8,128)(2,1)} %all-gather.5.cloned.1.call-done, bf16[1408,2048]{1,0:T(8,128)(2,1)} %bitcast.45), kind=kOutput, calls=%fused_computation.71 | convolution fusion | flops 1476395008 | bytes 8257536 | tf_op jit(solution)/shard_map/dot_general | solution.py:336
  303.3 9.1 %convolution_convert_fusion = bf16[256,2048]{1,0:T(8,128)(2,1)} fusion(bf16[1408,2048]{1,0:T(8,128)(2,1)} %bitcast.51, bf16[256,2048]{1,0:T(8,128)(2,1)S(1)} %copy-done.3, bf16[1408,2048]{1,0:T(8,128)(2,1)} %bitcast.48, f32[256,1408]{1,0:T(8,128)S(1)} %fusion.35), kind=kOutput, calls=%fused_computation.12 | convolution fusion | flops 2955476992 | bytes 15073280 | tf_op jit(solution)/shard_map/dot_general | solution.py:339
  312.7 15.1 %all-gather.3.cloned.1.call-done = bf16[256,2048]{1,0:T(8,128)(2,1)} async-done(((bf16[64,2048]{1,0:T(8,128)(2,1)}), bf16[256,2048]{1,0:T(8,128)(2,1)}) %all-gather.3.cloned.1.call-update) | async-done | bytes 1048592 | tf_op jit(solution)/shard_map/all_gather | solution.py:355
  327.9 4.9 %fusion.34 = f32[256,1408]{1,0:T(8,128)S(1)} fusion(bf16[256,2048]{1,0:T(8,128)(2,1)} %all-gather.3.cloned.1.call-done, bf16[1408,2048]{1,0:T(8,128)(2,1)} %bitcast.46), kind=kOutput, calls=%fused_computation.70 | convolution fusion | flops 1476395008 | bytes 8257536 | tf_op jit(solution)/shard_map/dot_general | solution.py:336
  332.7 9.1 %convolution_convert_fusion.1 = bf16[256,2048]{1,0:T(8,128)(2,1)} fusion(bf16[1408,2048]{1,0:T(8,128)(2,1)} %bitcast.52, bf16[256,2048]{1,0:T(8,128)(2,1)S(1)} %copy-done.2, bf16[1408,2048]{1,0:T(8,128)(2,1)} %bitcast.49, f32[256,1408]{1,0:T(8,128)S(1)} %fusion.34), kind=kOutput, calls=%fused_computation.13 | convolution fusion | flops 2955476992 | bytes 15073280 | tf_op jit(solution)/shard_map/dot_general | solution.py:339
  341.8 8.3 %shard_map.104.refs_0_ = bf16[2,2048,1408]{2,1,0:T(8,128)(2,1)} custom-call(bf16[1408,2048]{1,0:T(8,128)(2,1)} %bitcast.56), custom_call_target="tpu_custom_call" | custom-call | bytes 11534336 | tf_op jit(solution)/shard_map/pallas_call | solution.py:291
  350.1 8.3 %shard_map.105 = bf16[2,2048,1408]{2,1,0:T(8,128)(2,1)} custom-call(bf16[1408,2048]{1,0:T(8,128)(2,1)} %bitcast.53, bf16[2,2048,1408]{2,1,0:T(8,128)(2,1)} %shard_map.104.refs_0_), custom_call_target="tpu_custom_call", output_to_operand_aliasing={{}: (1, {})} | custom-call | bytes 11534336 | tf_op jit(solution)/shard_map/pallas_call | solution.py:291
  358.4 8.2 %shard_map.103 = bf16[2,2048,1408]{2,1,0:T(8,128)(2,1)} custom-call(bf16[1408,2048]{1,0:T(8,128)(2,1)} %bitcast.50, bf16[2,2048,1408]{2,1,0:T(8,128)(2,1)} %shard_map.101.refs_0_), custom_call_target="tpu_custom_call", output_to_operand_aliasing={{}: (1, {})} | custom-call | bytes 11534336 | tf_op jit(solution)/shard_map/pallas_call | solution.py:291
  366.6 8.2 %shard_map.102 = bf16[2,2048,1408]{2,1,0:T(8,128)(2,1)} custom-call(bf16[1408,2048]{1,0:T(8,128)(2,1)} %bitcast.47, bf16[2,2048,1408]{2,1,0:T(8,128)(2,1)} %shard_map.100.refs_0_), custom_call_target="tpu_custom_call", output_to_operand_aliasing={{}: (1, {})} | custom-call | bytes 11534336 | tf_op jit(solution)/shard_map/pallas_call | solution.py:291
  376.0 8.7 %reduce-scatter.9.cloned.1.call-done = bf16[64,2048]{1,0:T(8,128)(2,1)} async-done(((bf16[256,2048]{1,0:T(8,128)(2,1)}), bf16[64,2048]{1,0:T(8,128)(2,1)}) %reduce-scatter.9.cloned.1.call-update) | async-done | bytes 262160 | tf_op jit(solution)/shard_map/reduce_scatter | solution.py:340
  (45 shorter events, 18.2 us)
Async XLA Ops:
  7.2 235.3 %reduce-scatter.5.cloned.1.call-start = ((), (), s32[]{:S(2)}) async-start(), calls=%async_computation.4 | async-start | bytes 1310720 | tf_op jit(solution)/shard_map/reduce_scatter | solution.py:340
  23.9 3.0 copy-start
  209.4 58.8 %reduce-scatter.7.cloned.1.call-start = ((), (), s32[]{:S(2)}) async-start(), calls=%async_computation.5 | async-start | bytes 1310720 | tf_op jit(solution)/shard_map/reduce_scatter | solution.py:340
  224.7 73.8 %all-gather.5.cloned.1.call-start = ((), (), s32[]{:S(2)}) async-start(), calls=%async_computation.8 | async-start | bytes 1310720 | tf_op jit(solution)/shard_map/all_gather | solution.py:355
  233.0 8.3 %copy-start.1 = (f32[2,2048]{1,0:T(2,128)S(1)}, f32[2,2048]{1,0:T(2,128)}, u32[]{:S(2)}) copy-start(f32[2,2048]{1,0:T(2,128)} %param.11) | copy-start | bytes 49156
  271.8 56.0 %all-gather.3.cloned.1.call-start = ((), (), s32[]{:S(2)}) async-start(), calls=%async_computation.6 | async-start | bytes 1310720 | tf_op jit(solution)/shard_map/all_gather | solution.py:355
  272.7 102.1 %reduce-scatter.11.cloned.1.call-start = ((), (), s32[]{:S(2)}) async-start(), calls=%async_computation.9 | async-start | bytes 1310720 | tf_op jit(solution)/shard_map/reduce_scatter | solution.py:340
  298.5 4.9 %copy-start.3 = (bf16[256,2048]{1,0:T(8,128)(2,1)S(1)}, bf16[256,2048]{1,0:T(8,128)(2,1)}, u32[]{:S(2)}) copy-start(bf16[256,2048]{1,0:T(8,128)(2,1)} %all-gather.5.cloned.1.call-done) | copy-start | bytes 3145732
  312.4 72.2 %reduce-scatter.9.cloned.1.call-start = ((), (), s32[]{:S(2)}) async-start(), calls=%async_computation.7 | async-start | bytes 1310720 | tf_op jit(solution)/shard_map/reduce_scatter | solution.py:340
  327.9 4.9 %copy-start.2 = (bf16[256,2048]{1,0:T(8,128)(2,1)S(1)}, bf16[256,2048]{1,0:T(8,128)(2,1)}, u32[]{:S(2)}) copy-start(bf16[256,2048]{1,0:T(8,128)(2,1)} %all-gather.3.cloned.1.call-done) | copy-start | bytes 3145732
Sparse Core Ops, SparseCore 0:
  209.5 30.4 reduce-scatter.4
  242.3 25.7 reduce-scatter.6
  271.9 26.4 all-gather.4
  300.5 27.3 all-gather.2
  330.0 26.6 reduce-scatter.10
  358.8 25.7 reduce-scatter.8
